TPU v7x, 32 devices: a whole 2x2x4 slice. The times are simulated.
32 devices in a mesh: sp: 8 (over z, y), dp: 4 (over x, core).
Axes of the slice: x: 2, y: 2, z: 4, core: 2. Of those that a mesh axis runs over, the one named last changes fastest.
Arguments:
- out_cotangent: bfloat16 [4, 2048, 2048], P('dp', 'sp'), may hold values from -6 to 6
- value_pre: bfloat16 [4, 2048, 2048], P('dp', 'sp'), may hold values from -8 to 8
- gate_pre: bfloat16 [4, 2048, 2048], P('dp', 'sp'), may hold values from -8 to 8
- out_weight: bfloat16 [2048, 2048], P('dp'), may hold values from -0.125 to 0.125
- conv_kernel: bfloat16 [31, 2048], P(None, 'sp'), may hold values from -6 to 6
- norm_gain: bfloat16 [2048], P('sp'), may hold values from 0.099609375 to 1.8984375
Outputs:
- grad_value: bfloat16 [4, 2048, 2048], P('dp', 'sp')
- grad_gate: bfloat16 [4, 2048, 2048], P('dp', 'sp')
- grad_out_weight: float32 [2048, 2048], P(('sp', 'dp'))
- grad_kernel: float32 [31, 2048], P(None, 'sp')
- grad_gain: float32 [2048], P('sp')
All inputs are finite; a program needn't handle non-finite values.
Results may differ from a plain program's by a relative error of at most 0.011.
Values may be sent and summed in bfloat16 or wider, within the bound.
No kernel may reach another device: no remote copies, remote signals or barrier semaphores. Data moves between devices by JAX's collectives and lax.ppermute only.
A program may use at most 128 MiB of HBM per device.

v0:
```python
import jax
import jax.numpy as jnp
from jax import lax
from jax.sharding import PartitionSpec as P

epsilon = 1e-05


def passed_along(value, axis, steps):
    count = lax.axis_size(axis)
    initial, last = (max(0, -steps), min(count, count - steps))
    return lax.ppermute(value, axis, [(source, source + steps) for source in range(initial, last)])


def gated_forward(values_in, gates_in):
    return (values_in.astype(jnp.float32) * jax.nn.sigmoid(gates_in.astype(jnp.float32))).astype(
        jnp.bfloat16
    )


def gated_backward(grad_gated, values_in, gates_in):
    sigmoid_gate = jax.nn.sigmoid(gates_in.astype(jnp.float32))
    grad_float = grad_gated.astype(jnp.float32)
    grad_values = (grad_float * sigmoid_gate).astype(jnp.bfloat16)
    grad_gates = (
        grad_float * values_in.astype(jnp.float32) * sigmoid_gate * (1.0 - sigmoid_gate)
    ).astype(jnp.bfloat16)
    return (grad_values, grad_gates)


def local_sums(first, second):
    return (first, second)


def mechanism(
    gated, front_rows, grad_act, kernel, gain, channel_count, moments_fn, grad_moments_fn, after_fn
):
    taps_count = kernel.shape[0]
    row_count = gated.shape[0]
    taps_float = kernel.astype(jnp.float32)
    gain_float = gain.astype(jnp.float32)
    extended = jnp.concatenate([front_rows, gated], axis=0).astype(jnp.float32)
    conv = jnp.zeros((row_count, gated.shape[1]), jnp.float32)
    for offset in range(taps_count):
        begin = taps_count - 1 - offset
        conv = conv + taps_float[offset] * extended[begin : begin + row_count]
    total, squares = moments_fn(jnp.sum(conv, axis=1), jnp.sum(conv * conv, axis=1))
    centre = (total / channel_count)[:, None]
    variance = (squares / channel_count)[:, None] - centre * centre
    inv_scale = lax.rsqrt(variance + epsilon)
    centred = (conv - centre) * inv_scale
    normed = centred * gain_float
    sig_norm = jax.nn.sigmoid(normed)
    activation = (normed * sig_norm).astype(jnp.bfloat16)
    grad_normed = grad_act.astype(jnp.float32) * sig_norm * (1.0 + normed * (1.0 - sig_norm))
    gain_part = jnp.sum(grad_normed * centred, axis=0)
    grad_centred = grad_normed * gain_float
    first, second = grad_moments_fn(
        jnp.sum(grad_centred, axis=1), jnp.sum(grad_centred * centred, axis=1)
    )
    grad_conv = (
        grad_centred
        - (first / channel_count)[:, None]
        - centred * (second / channel_count)[:, None]
    ) * inv_scale
    grad_extended = jnp.concatenate([grad_conv, after_fn(grad_conv, taps_count)], axis=0)
    grad_gated = jnp.zeros(grad_conv.shape, jnp.float32)
    kernel_rows = []
    for offset in range(taps_count):
        grad_gated = grad_gated + taps_float[offset] * grad_extended[offset : offset + row_count]
        begin = taps_count - 1 - offset
        kernel_rows.append(jnp.sum(grad_conv * extended[begin : begin + row_count], axis=0))
    return (activation, grad_gated.astype(jnp.bfloat16), jnp.stack(kernel_rows, axis=0), gain_part)


def shards(out_cotangent, value_pre, gate_pre, out_weight, conv_kernel, norm_gain):
    cotangent = out_cotangent[0]
    values_in = value_pre[0]
    gates_in = gate_pre[0]
    row_count = cotangent.shape[0]
    taps_count = conv_kernel.shape[0]
    width_all = cotangent.shape[1]
    grad_act = lax.dot_general(
        cotangent,
        lax.all_gather(out_weight, "dp", axis=0, tiled=True),
        (((1,), (1,)), ((), ())),
        preferred_element_type=jnp.float32,
    ).astype(jnp.bfloat16)
    kernel_all, gain_all = (
        lax.all_gather(conv_kernel, "sp", axis=1, tiled=True),
        lax.all_gather(norm_gain, "sp", axis=0, tiled=True),
    )
    gated = gated_forward(values_in, gates_in)
    front_rows = passed_along(gated[row_count - taps_count + 1 :], "sp", 1)

    def later_margin(grad_conv, count_taps):
        return passed_along(grad_conv[: count_taps - 1], "sp", -1)

    activation, grad_gated, kernel_full, gain_full = mechanism(
        gated,
        front_rows,
        grad_act,
        kernel_all,
        gain_all,
        float(width_all),
        local_sums,
        local_sums,
        later_margin,
    )
    kernel_part, gain_part = (
        lax.psum_scatter(kernel_full, "sp", scatter_dimension=1, tiled=True),
        lax.psum_scatter(gain_full, "sp", scatter_dimension=0, tiled=True),
    )
    grad_values, grad_gates = gated_backward(grad_gated, values_in, gates_in)
    token_total = lax.axis_size("sp") * lax.axis_size("dp") * row_count
    factor = float(token_total) ** (-0.5)
    kernel_sum, gain_sum = lax.psum((kernel_part, gain_part), "dp")
    weight_sum = lax.psum_scatter(
        lax.dot_general(
            activation, cotangent, (((0,), (0,)), ((), ())), preferred_element_type=jnp.float32
        ),
        ("sp", "dp"),
        scatter_dimension=0,
        tiled=True,
    )
    return (
        grad_values[None],
        grad_gates[None],
        weight_sum * factor,
        kernel_sum * factor,
        gain_sum * factor,
    )


def solution(mesh):
    placed = (
        P("dp", "sp", None),
        P("dp", "sp", None),
        P("dp", "sp", None),
        P("dp", None),
        P(None, "sp"),
        P("sp"),
    )
    return jax.shard_map(
        shards,
        mesh=mesh,
        in_specs=placed,
        out_specs=(
            P("dp", "sp", None),
            P("dp", "sp", None),
            P(("sp", "dp"), None),
            P(None, "sp"),
            P("sp"),
        ),
        check_vma=False,
    )
```

profile of v0, /device:TPU:0, one launch (start us, length us, event | category | flops | bytes accessed | tf_op | source)
XLA Modules:
  0.0 355.4 jit_solution(7777059635659343137)
XLA Ops:
  7.2 0.0 copy-start
  7.2 0.0 copy-start.4
  7.2 0.0 copy-start.6
  7.2 0.0 all-gather.3.cloned.1.call-start
  7.3 0.7 all-gather.3.cloned.1.call-update
  7.9 0.0 copy-start.24
  8.0 0.0 copy-start.26
  8.0 0.0 reduce-scatter.5.cloned.1.call-start
  8.0 0.5 copy-done.4
  8.5 0.3 copy-done.6
  8.8 0.6 fusion.93
  9.4 4.9 %collective-permute-start = (bf16[30,2048]{1,0:T(8,128)(2,1)S(1)}, bf16[30,2048]{1,0:T(8,128)(2,1)S(1)}, u32[]{:S(2)}, u32[]{:S(2)}) collective-permute-start(bf16[30,2048]{1,0:T(8,128)(2,1)S(1)} %slice.439), channel_id=1, source_target_pairs={{0,4},{4,8},{8,12},{12,16},{16,20},{20,24},{24,28},{1,5},{5,9},{9,... | collective-permute-start | bytes 368648 | tf_op jit(solution)/shard_map/ppermute | solution.py:12
  14.3 0.0 copy-done.24
  14.3 30.9 %all_gather.9 = bf16[31,2048]{1,0:T(8,128)(2,1)S(1)} all-gather(bf16[31,256]{1,0:T(8,128)(2,1)S(1)} %copy-done.24), channel_id=1, replica_groups=mesh['sp'=8,'dp'=4] {'sp'}, dimensions={1}, use_global_device_ids=true | all-gather | bytes 142848 | tf_op jit(solution)/shard_map/all_gather | solution.py:90
  45.3 0.1 fusion.110
  45.4 0.0 copy-start.7
  45.4 0.0 copy-start.9
  45.4 0.1 fusion.111
  45.6 18.3 %all-gather = bf16[8,1,256]{2,1,0:T(2,128)(2,1)S(1)} all-gather(bf16[1,1,256]{2,1,0:T(2,128)(2,1)S(1)} %reshape.43), channel_id=1, replica_groups=mesh['sp'=8,'dp'=4] {'sp'}, dimensions={0}, use_global_device_ids=true | all-gather | bytes 4608 | tf_op jit(solution)/shard_map/all_gather | solution.py:91
  63.9 0.0 collective-permute-done
  63.9 0.3 maximum_convert_fusion
  64.2 11.8 %fusion.108 = (f32[256]{0:T(256)S(1)}, f32[256]{0:T(256)S(1)}, f32[256,2048]{1,0:T(8,128)}) fusion(f32[286,2048]{1,0:T(8,128)S(1)} %maximum_convert_fusion, f32[2048]{0:T(1024)S(1)} %bitcast.154, f32[2048]{0:T(1024)S(1)} %bitcast.152, f32[2048]{0:T(1024)S(1)} %bitcast.150, f32[2048]{0:T(1024)S(1)} %bitcast.148, f32[2048]{0:T(1024)S(1)} %bitcast.146, ...), kind=kLoop, calls=%fused_computation.221 | loop fusion | flops 33553920 | bytes 67364864 | tf_op jit(solution)/shard_map/reduce_sum | solution.py:47
  76.2 0.6 broadcast_multiply_fusion.5
  76.8 0.0 copy-start.23
  76.8 8.1 %multiply_reduce_fusion = (f32[2048]{0:T(1024)}, f32[256]{0:T(256)S(1)}, f32[256]{0:T(256)S(1)}, f32[256,2048]{1,0:T(8,128)S(1)}) fusion(f32[256,2048]{1,0:T(8,128)} %get-tuple-element.46, f32[256]{0:T(256)} %get-tuple-element.79, f32[256]{0:T(256)} %get-tuple-element.78, f32[2048]{0:T(1024)S(1)} %bitcast.91, ...), kind=kOutput, calls=%fused_computation.162 | convolution fusion | flops 2157442560 | bytes 13651968 | tf_op jit(solution)/shard_map/dot_general | solution.py:83
  84.9 6.8 %multiply_reduce_fusion.1 = (f32[2048]{0:T(1024)}, f32[2048]{0:T(1024)}, f32[2048]{0:T(1024)}, f32[2048]{0:T(1024)}, f32[2048]{0:T(1024)}, /*index=5*/f32[2048]{...) fusion(f32[286,2048]{1,0:T(8,128)S(1)} %maximum_convert_fusion,, ...), kind=kLoop, calls=%fused_computation.163 | loop fusion | flops 22507520 | bytes 44199936 | tf_op jit(solution)/shard_map/reduce_sum | solution.py:72
  91.7 4.8 %multiply_reduce_fusion.19 = (f32[2048]{0:T(1024)}, f32[2048]{0:T(1024)}, f32[2048]{0:T(1024)}, f32[2048]{0:T(1024)}, f32[2048]{0:T(1024)}, /*index=5*/f32[2048]...) fusion(f32[256,2048]{1,0:T(8,128)S(1)} %get-tuple-element.43, ...), kind=kLoop, calls=%fused_computation.181 | loop fusion | flops 13604864 | bytes 29466624 | tf_op jit(solution)/shard_map/reduce_sum | solution.py:72
  96.5 6.1 %stack.127 = f32[31,2048]{1,0:T(8,128)} concatenate(f32[1,2048]{1,0:T(1,128)} %bitcast.186, f32[1,2048]{1,0:T(1,128)} %bitcast.185, f32[1,2048]{1,0:T(1,128)} %bitcast.184, f32[1,2048]{1,0:T(1,128)} %bitcast.183, f32[1,2048]{1,0:T(1,128)} %bitcast.182, f32[1,2048]{1,0:T(1,128)} %bitcast.181, f32[1,2048]{1,0:T(1,128)} %bitcast.180, f32[1,2048]{1,0:T(1,128)} %bitcast.179, ...), dimensions={0} | concatenate | bytes 507904 | tf_op jit(solution)/shard_map/stack | solution.py:73
  102.6 0.0 reduce-scatter.5.cloned.1.call-update
  102.6 0.2 reduce-scatter.3.cloned.1.call-start
  102.8 10.0 %fusion.98 = f32[2048,2048]{1,0:T(8,128)} fusion(f32[256,2048]{1,0:T(8,128)} %get-tuple-element.46, bf16[1,256,2048]{2,1,0:T(8,128)(2,1)S(1)} %copy-done, f32[2048]{0:T(1024)S(1)} %bitcast.93, f32[256]{0:T(256)} %get-tuple-element.79, f32[256]{0:T(256)} %get-tuple-element.78), kind=kOutput, calls=%fused_computation.204 | convolution fusion | flops 2151677952 | bytes 19933184 | tf_op jit(solution)/shard_map/dot_general | solution.py:119
  112.9 0.0 reduce-scatter.3.cloned.1.call-update
  112.9 1.6 copy-done.2
  114.5 1.3 collective-permute-start.1
  115.8 1.2 dynamic-slice
  117.7 20.8 %all-reduce = f32[2048]{0:T(1024)} all-reduce(f32[2048]{0:T(1024)} %get-tuple-element.36), channel_id=4, replica_groups=mesh['sp'=8,'dp'=4] {'sp'}, use_global_device_ids=true, to_apply=%region_39.0.clone | all-reduce | flops 2048 | bytes 16384
  138.5 1.3 dynamic-slice.1
  139.8 0.0 collective-permute-done.1
  139.8 0.0 copy-done.8
  139.9 18.0 %fusion.99 = (bf16[1,256,2048]{2,1,0:T(8,128)(2,1)}, bf16[256,2048]{1,0:T(8,128)(2,1)S(1)}) fusion(bf16[1,256,2048]{2,1,0:T(8,128)(2,1)} %param.7, bf16[1,256,2048]{2,1,0:T(8,128)(2,1)} %param.8, f32[30,2048]{1,0:T(8,128)} %collective-permute-done.1, f32[256,2048]{1,0:T(8,128)S(1)} %copy-done.2, f32[2048]{0:T(1024)} %bitcast.155, f32[2048]{0:T(1024)} %bitcast.153, ...), kind=kLoop, calls=%fused_computation.205 | loop fusion | flops 54001664 | bytes 6791168 | tf_op jit(solution)/shard_map/broadcast_in_dim | solution.py:128
  157.9 0.0 copy-start.25
  157.9 1.6 fusion.100
  159.5 3.2 reduce-scatter.5.cloned.1.call-done
  162.6 11.7 %all-reduce.1 = (f32[31,256]{1,0:T(8,128)S(1)}, f32[256]{0:T(256)S(1)}) all-reduce(f32[31,256]{1,0:T(8,128)} %reduce-scatter.5.cloned.1.call-done, f32[256]{0:T(256)S(1)} %copy-done.25), channel_id=1, replica_groups=mesh['sp'=8,'dp'=4] {'dp'}, use_global_device_ids=true, to_apply=%region_37.0 | all-reduce | flops 8192 | bytes 65536 | tf_op jit(solution)/shard_map/psum | solution.py:117
  174.3 0.6 broadcast_multiply_fusion.2
  174.9 0.6 broadcast_multiply_fusion.1
  175.5 171.5 %reduce-scatter.3.cloned.1.call-done = f32[64,2048]{1,0:T(8,128)} async-done(((f32[2048,2048]{1,0:T(8,128)}), f32[64,2048]{1,0:T(8,128)}) %reduce-scatter.3.cloned.1.call-update) | async-done | bytes 524304 | tf_op jit(solution)/shard_map/reduce_scatter | solution.py:118
  347.0 1.9 broadcast_multiply_fusion
  (46 shorter events, 0.2 us)
Async XLA Ops:
  7.2 69.6 %copy-start = (bf16[1,256,2048]{2,1,0:T(8,128)(2,1)S(1)}, bf16[1,256,2048]{2,1,0:T(8,128)(2,1)}, u32[]{:S(2)}) copy-start(bf16[1,256,2048]{2,1,0:T(8,128)(2,1)} %param.6) | copy-start | bytes 3145732
  7.2 1.3 copy-start.4
  7.2 1.6 copy-start.6
  7.2 69.6 %all-gather.3.cloned.1.call-start = ((), (), s32[]{:S(2)}) async-start(), calls=%async_computation.2 | async-start | bytes 10485760 | tf_op jit(solution)/shard_map/all_gather | solution.py:85
  7.9 6.4 %copy-start.24 = (bf16[31,256]{1,0:T(8,128)(2,1)S(1)}, bf16[31,256]{1,0:T(8,128)(2,1)}, u32[]{:S(2)}) copy-start(bf16[31,256]{1,0:T(8,128)(2,1)} %param.10) | copy-start | bytes 47620
  8.0 37.5 %copy-start.26 = (bf16[256]{0:T(256)(128)(2,1)S(1)}, bf16[256]{0:T(256)(128)(2,1)}, u32[]{:S(2)}) copy-start(bf16[256]{0:T(256)(128)(2,1)} %param.11) | copy-start | bytes 1540
  8.0 154.7 %reduce-scatter.5.cloned.1.call-start = ((), (), s32[]{:S(2)}) async-start(), calls=%async_computation.4 | async-start | bytes 294912 | tf_op jit(solution)/shard_map/reduce_scatter | solution.py:111
  9.4 54.5 %collective-permute-start = (bf16[30,2048]{1,0:T(8,128)(2,1)S(1)}, bf16[30,2048]{1,0:T(8,128)(2,1)S(1)}, u32[]{:S(2)}, u32[]{:S(2)}) collective-permute-start(bf16[30,2048]{1,0:T(8,128)(2,1)S(1)} %slice.439), channel_id=1, source_target_pairs={{0,4},{4,8},{8,12},{12,16},{16,20},{20,24},{24,28},{1,5},{5,9},{9,... | collective-permute-start | bytes 368648 | tf_op jit(solution)/shard_map/ppermute | solution.py:12
  45.4 30.7 %copy-start.7 = (f32[1,2048]{1,0:T(1,128)}, f32[1,2048]{1,0:T(1,128)S(1)}, u32[]{:S(2)}) copy-start(f32[1,2048]{1,0:T(1,128)S(1)} %get-tuple-element.64) | copy-start | bytes 24580
  45.4 30.6 %copy-start.9 = (f32[1,2048]{1,0:T(1,128)}, f32[1,2048]{1,0:T(1,128)S(1)}, u32[]{:S(2)}) copy-start(f32[1,2048]{1,0:T(1,128)S(1)} %get-tuple-element.65) | copy-start | bytes 24580
  45.5 30.5 %copy-start.10 = (f32[1,2048]{1,0:T(1,128)}, f32[1,2048]{1,0:T(1,128)S(1)}, u32[]{:S(2)}) copy-start(f32[1,2048]{1,0:T(1,128)S(1)} %get-tuple-element.66) | copy-start | bytes 24580
  45.5 30.5 %copy-start.11 = (f32[1,2048]{1,0:T(1,128)}, f32[1,2048]{1,0:T(1,128)S(1)}, u32[]{:S(2)}) copy-start(f32[1,2048]{1,0:T(1,128)S(1)} %get-tuple-element.67) | copy-start | bytes 24580
  45.5 30.5 %copy-start.12 = (f32[1,2048]{1,0:T(1,128)}, f32[1,2048]{1,0:T(1,128)S(1)}, u32[]{:S(2)}) copy-start(f32[1,2048]{1,0:T(1,128)S(1)} %get-tuple-element.68) | copy-start | bytes 24580
  45.5 30.5 %copy-start.13 = (f32[1,2048]{1,0:T(1,128)}, f32[1,2048]{1,0:T(1,128)S(1)}, u32[]{:S(2)}) copy-start(f32[1,2048]{1,0:T(1,128)S(1)} %get-tuple-element.69) | copy-start | bytes 24580
  45.5 30.5 %copy-start.14 = (f32[1,2048]{1,0:T(1,128)}, f32[1,2048]{1,0:T(1,128)S(1)}, u32[]{:S(2)}) copy-start(f32[1,2048]{1,0:T(1,128)S(1)} %get-tuple-element.70) | copy-start | bytes 24580
  45.5 30.5 %copy-start.15 = (f32[1,2048]{1,0:T(1,128)}, f32[1,2048]{1,0:T(1,128)S(1)}, u32[]{:S(2)}) copy-start(f32[1,2048]{1,0:T(1,128)S(1)} %get-tuple-element.71) | copy-start | bytes 24580
  45.6 30.5 %copy-start.16 = (f32[1,2048]{1,0:T(1,128)}, f32[1,2048]{1,0:T(1,128)S(1)}, u32[]{:S(2)}) copy-start(f32[1,2048]{1,0:T(1,128)S(1)} %get-tuple-element.72) | copy-start | bytes 24580
  45.6 30.5 %copy-start.17 = (f32[1,2048]{1,0:T(1,128)}, f32[1,2048]{1,0:T(1,128)S(1)}, u32[]{:S(2)}) copy-start(f32[1,2048]{1,0:T(1,128)S(1)} %get-tuple-element.73) | copy-start | bytes 24580
  45.6 30.5 %copy-start.18 = (f32[1,2048]{1,0:T(1,128)}, f32[1,2048]{1,0:T(1,128)S(1)}, u32[]{:S(2)}) copy-start(f32[1,2048]{1,0:T(1,128)S(1)} %get-tuple-element.74) | copy-start | bytes 24580
  45.6 30.5 %copy-start.19 = (f32[1,2048]{1,0:T(1,128)}, f32[1,2048]{1,0:T(1,128)S(1)}, u32[]{:S(2)}) copy-start(f32[1,2048]{1,0:T(1,128)S(1)} %get-tuple-element.75) | copy-start | bytes 24580
  45.6 30.5 %copy-start.20 = (f32[1,2048]{1,0:T(1,128)}, f32[1,2048]{1,0:T(1,128)S(1)}, u32[]{:S(2)}) copy-start(f32[1,2048]{1,0:T(1,128)S(1)} %get-tuple-element.76) | copy-start | bytes 24580
  45.6 30.5 %copy-start.21 = (f32[1,2048]{1,0:T(1,128)}, f32[1,2048]{1,0:T(1,128)S(1)}, u32[]{:S(2)}) copy-start(f32[1,2048]{1,0:T(1,128)S(1)} %get-tuple-element.77) | copy-start | bytes 24580
  76.8 8.1 %copy-start.3 = (f32[256,2048]{1,0:T(8,128)S(1)}, f32[256,2048]{1,0:T(8,128)}, u32[]{:S(2)}) copy-start(f32[256,2048]{1,0:T(8,128)} %get-tuple-element.46) | copy-start | bytes 6291460
  76.8 8.1 %copy-start.22 = (f32[256]{0:T(256)S(1)}, f32[256]{0:T(256)}, u32[]{:S(2)}) copy-start(f32[256]{0:T(256)} %get-tuple-element.78) | copy-start | bytes 3076
  76.8 8.1 %copy-start.23 = (f32[256]{0:T(256)S(1)}, f32[256]{0:T(256)}, u32[]{:S(2)}) copy-start(f32[256]{0:T(256)} %get-tuple-element.79) | copy-start | bytes 3076
  91.7 4.8 %copy-start.1 = (f32[256,2048]{1,0:T(8,128)}, f32[256,2048]{1,0:T(8,128)S(1)}, u32[]{:S(2)}) copy-start(f32[256,2048]{1,0:T(8,128)S(1)} %get-tuple-element.43) | copy-start | bytes 6291460
  102.6 244.3 %reduce-scatter.3.cloned.1.call-start = ((), (), s32[]{:S(2)}) async-start(), calls=%async_computation.3 | async-start | bytes 17301504 | tf_op jit(solution)/shard_map/reduce_scatter | solution.py:118
  112.9 1.6 copy-start.2
  112.9 27.0 %copy-start.8 = (f32[1,2048]{1,0:T(1,128)S(1)}, f32[1,2048]{1,0:T(1,128)}, u32[]{:S(2)}) copy-start(f32[1,2048]{1,0:T(1,128)} %copy-done.7) | copy-start | bytes 24580
  114.5 25.3 %collective-permute-start.1 = (f32[30,2048]{1,0:T(8,128)S(1)}, f32[30,2048]{1,0:T(8,128)}, u32[]{:S(2)}, u32[]{:S(2)}) collective-permute-start(f32[30,2048]{1,0:T(8,128)S(1)} %slice.501), channel_id=1, source_target_pairs={{4,0},{8,4},{12,8},{16,12},{20,16},{24,20},{28,24},{5,1},{9,5},{13... | collective-permute-start | bytes 737288 | tf_op jit(solution)/shard_map/ppermute | solution.py:12
  139.8 18.1 %copy-start.5 = (bf16[1,256,2048]{2,1,0:T(8,128)(2,1)S(1)}, bf16[1,256,2048]{2,1,0:T(8,128)(2,1)}, u32[]{:S(2)}) copy-start(bf16[1,256,2048]{2,1,0:T(8,128)(2,1)} %param.8) | copy-start | bytes 3145732
  157.9 4.7 %copy-start.25 = (f32[256]{0:T(256)S(1)}, f32[256]{0:T(256)}, u32[]{:S(2)}) copy-start(f32[256]{0:T(256)} %dynamic-slice.1) | copy-start | bytes 3076
Sparse Core Ops, SparseCore 0:
  9.6 60.9 all-gather.2
  102.7 59.8 reduce-scatter.4
  164.9 181.9 reduce-scatter.2
where the time goes:
time: 357 us; the launch traced here: 355 us
  waiting for transfers between devices  175 us (49%)
  blocking collectives  81.7 us (23%)
  other arithmetic  47.5 us (13%)
  matrix products  18.1 us (5%)
  between operations  14.8 us (4%)
  local copies, waits for them, and re-layouts  11.4 us (3%)
  starting transfers between devices  6.5 us (2%)
    reduce_scatter x1, waiting for transfers between devices, shards(): lax.psum_scatter(lax.dot_general(activation, cotangent, (((0,), (0,)), ((...  171 us
    all_gather x1, blocking collectives, shards(): lax.all_gather(conv_kernel, 'sp', axis=1, tiled=True)  30.9 us
    unnamed x1, blocking collectives  20.8 us
    all_gather x1, blocking collectives, shards(): lax.all_gather(norm_gain, 'sp', axis=0, tiled=True)  18.3 us
    broadcast_in_dim x1, other arithmetic, shards(): grad_gates[None]  18 us
    reduce_sum x1, other arithmetic, mechanism(): jnp.sum(conv, axis=1)  11.8 us
    psum x1, blocking collectives, shards(): kernel_sum, gain_sum = lax.psum((kernel_part, gain_part), 'dp')  11.7 us
    reduce_sum x2, other arithmetic, mechanism(): jnp.sum(grad_conv * extended[begin:begin + row_count], axis=0)  11.6 us
  transfers between devices with their start and end apart: 5, of which 2 were waited for; matrix products, arithmetic and copies ran while one was open for 13% of the time, Pallas kernels for 0%

commit v1 on v0

v1 whole, which is shorter than its diff:
```python
import jax
import jax.numpy as jnp
from jax import lax
from jax.sharding import PartitionSpec as P

epsilon = 1e-05
CORES = 2


def chip_shift(value, chips, cores, steps):
    pairs = [
        (chip * cores + core, (chip + steps) % chips * cores + core)
        for chip in range(chips)
        for core in range(cores)
    ]
    return lax.ppermute(value, "dp", pairs)


def core_swap(value, chips, cores):
    return lax.ppermute(value, "dp", [(i, i ^ 1) for i in range(chips * cores)])


def bit_swap(value, axis, bit):
    count = lax.axis_size(axis)
    return lax.ppermute(value, axis, [(i, i ^ (1 << bit)) for i in range(count)])


def passed_along(value, axis, steps):
    count = lax.axis_size(axis)
    initial, last = (max(0, -steps), min(count, count - steps))
    return lax.ppermute(value, axis, [(source, source + steps) for source in range(initial, last)])


def gathered(value, axis):
    count = lax.axis_size(axis)
    bits = count.bit_length() - 1
    me = lax.axis_index(axis)
    whole = value[None]
    for bit in range(bits):
        other = bit_swap(whole, axis, bit)
        mine_first = ((me >> bit) & 1) == 0
        whole = jnp.where(
            mine_first,
            jnp.concatenate([whole, other], axis=0),
            jnp.concatenate([other, whole], axis=0),
        )
    return whole.transpose(1, 0, 2).reshape(value.shape[0], -1)


def gated_forward(values_in, gates_in):
    return (values_in.astype(jnp.float32) * jax.nn.sigmoid(gates_in.astype(jnp.float32))).astype(
        jnp.bfloat16
    )


def gated_backward(grad_gated, values_in, gates_in):
    sigmoid_gate = jax.nn.sigmoid(gates_in.astype(jnp.float32))
    grad_float = grad_gated.astype(jnp.float32)
    grad_values = (grad_float * sigmoid_gate).astype(jnp.bfloat16)
    grad_gates = (
        grad_float * values_in.astype(jnp.float32) * sigmoid_gate * (1.0 - sigmoid_gate)
    ).astype(jnp.bfloat16)
    return (grad_values, grad_gates)


def scattered_sum(parts, axis):
    count = lax.axis_size(axis)
    bits = count.bit_length() - 1
    me = lax.axis_index(axis)
    for bit in range(bits):
        mine = (me >> bit) & 1
        pairs = parts.reshape((parts.shape[0] // 2, 2) + parts.shape[1:])
        keep = lax.dynamic_index_in_dim(pairs, mine, axis=1, keepdims=False)
        send = lax.dynamic_index_in_dim(pairs, 1 - mine, axis=1, keepdims=False)
        parts = keep + bit_swap(send.astype(jnp.bfloat16), axis, bit).astype(jnp.float32)
    return parts[0]


def shards(out_cotangent, value_pre, gate_pre, out_weight, conv_kernel, norm_gain):
    cotangent = out_cotangent[0]
    values_in = value_pre[0]
    gates_in = gate_pre[0]
    row_count, width = cotangent.shape
    taps_count = conv_kernel.shape[0]
    margin = taps_count - 1
    sp_count, dp_count = lax.axis_size("sp"), lax.axis_size("dp")
    cores = CORES if dp_count % CORES == 0 else 1
    chips = dp_count // cores
    place = lax.axis_index("dp")
    chip, core = place // cores, place % cores
    width_float = float(width)

    small = gathered(jnp.concatenate([conv_kernel, norm_gain[None]], axis=0), "sp")
    front_rows = passed_along(
        gated_forward(values_in[row_count - margin :], gates_in[row_count - margin :]), "sp", 1
    )
    cots = [cotangent] + [chip_shift(cotangent, chips, cores, k) for k in range(1, chips)]
    weight_other = core_swap(out_weight, chips, cores)

    def times_weights(cot):
        dims = (((1,), (1,)), ((), ()))
        mine = lax.dot_general(cot, out_weight, dims, preferred_element_type=jnp.float32)
        other = lax.dot_general(cot, weight_other, dims, preferred_element_type=jnp.float32)
        mine, other = mine.astype(jnp.bfloat16), other.astype(jnp.bfloat16)
        return jnp.where(
            core == 0,
            jnp.concatenate([mine, other], axis=1),
            jnp.concatenate([other, mine], axis=1),
        )

    grad_act = jnp.zeros((row_count, width), jnp.bfloat16)
    for k in range(chips):
        piece = times_weights(cots[k])
        if k:
            piece = chip_shift(piece, chips, cores, -k)
        grad_act = lax.dynamic_update_slice(
            grad_act, piece, (0, (chip + k) % chips * piece.shape[1])
        )

    taps_float = small[:taps_count].astype(jnp.float32)
    gain_float = small[taps_count].astype(jnp.float32)
    gated = gated_forward(values_in, gates_in)
    extended = jnp.concatenate([front_rows, gated], axis=0).astype(jnp.float32)
    conv = jnp.zeros((row_count, width), jnp.float32)
    for offset in range(taps_count):
        begin = margin - offset
        conv = conv + taps_float[offset] * extended[begin : begin + row_count]
    centre = (jnp.sum(conv, axis=1) / width_float)[:, None]
    variance = (jnp.sum(conv * conv, axis=1) / width_float)[:, None] - centre * centre
    inv_scale = lax.rsqrt(variance + epsilon)
    centred = (conv - centre) * inv_scale
    normed = centred * gain_float
    sig_norm = jax.nn.sigmoid(normed)
    activation = (normed * sig_norm).astype(jnp.bfloat16)

    rows_out = width // (sp_count * dp_count)
    act_rows = activation.T.reshape(sp_count, chips, cores, rows_out, row_count)

    def for_chip(k):
        return lax.dynamic_index_in_dim(act_rows, (chip + k) % chips, axis=1, keepdims=False)

    acts = [for_chip(0)] + [
        chip_shift(for_chip(k), chips, cores, k) for k in range(1, chips)
    ]
    lefts, rights = [], []
    for act, cot in zip(acts, cots):
        lefts.append(lax.dynamic_index_in_dim(act, core, axis=1, keepdims=False))
        rights.append(cot)
        if cores > 1:
            others = lax.dynamic_index_in_dim(act, 1 - core, axis=1, keepdims=False)
            lefts.append(core_swap(others, chips, cores))
            rights.append(core_swap(cot, chips, cores))
    left = jnp.concatenate(lefts, axis=2).reshape(sp_count * rows_out, -1)
    right = jnp.concatenate(rights, axis=0)
    weight_part = lax.dot_general(
        left, right, (((1,), (0,)), ((), ())), preferred_element_type=jnp.float32
    )
    weight_sum = scattered_sum(weight_part.reshape(sp_count, rows_out, width), "sp")

    grad_normed = grad_act.astype(jnp.float32) * sig_norm * (1.0 + normed * (1.0 - sig_norm))
    gain_part = jnp.sum(grad_normed * centred, axis=0)
    grad_centred = grad_normed * gain_float
    first = jnp.sum(grad_centred, axis=1)
    second = jnp.sum(grad_centred * centred, axis=1)
    grad_conv = (
        grad_centred
        - (first / width_float)[:, None]
        - centred * (second / width_float)[:, None]
    ) * inv_scale
    kernel_rows = []
    for offset in range(taps_count):
        begin = margin - offset
        kernel_rows.append(jnp.sum(grad_conv * extended[begin : begin + row_count], axis=0))
    small_part = jnp.stack(kernel_rows + [gain_part], axis=0)
    small_part = lax.all_to_all(small_part, "sp", 1, 0, tiled=True)
    small_part = jnp.sum(small_part.reshape(sp_count, taps_count + 1, -1), axis=0)
    small_sum = jnp.sum(lax.all_gather(small_part, "dp"), axis=0)

    grad_extended = jnp.concatenate([grad_conv, passed_along(grad_conv[:margin], "sp", -1)], axis=0)
    grad_gated = jnp.zeros(grad_conv.shape, jnp.float32)
    for offset in range(taps_count):
        grad_gated = grad_gated + taps_float[offset] * grad_extended[offset : offset + row_count]
    grad_values, grad_gates = gated_backward(grad_gated.astype(jnp.bfloat16), values_in, gates_in)

    factor = float(sp_count * dp_count * row_count) ** (-0.5)
    return (
        grad_values[None],
        grad_gates[None],
        weight_sum * factor,
        small_sum[:taps_count] * factor,
        small_sum[taps_count] * factor,
    )


def solution(mesh):
    placed = (
        P("dp", "sp", None),
        P("dp", "sp", None),
        P("dp", "sp", None),
        P("dp", None),
        P(None, "sp"),
        P("sp"),
    )
    return jax.shard_map(
        shards,
        mesh=mesh,
        in_specs=placed,
        out_specs=(
            P("dp", "sp", None),
            P("dp", "sp", None),
            P(("sp", "dp"), None),
            P(None, "sp"),
            P("sp"),
        ),
        check_vma=False,
    )
```

time: 357 us -> 235 us (0.66)
  waiting for transfers between devices: 175 us -> 20.8 us
  other arithmetic: 47.5 us -> 125 us
  blocking collectives: 81.7 us -> 5.42 us
  starting transfers between devices: 6.5 us -> 33.9 us
  local copies, waits for them, and re-layouts: 11.4 us -> 33.2 us
  between operations: 14.8 us -> 1.3 us
    reduce_scatter x2 -> x0, waiting for transfers between devices: 175 us -> none  [the longest x1 171 us: shards(): lax.psum_scatter(lax.dot_general(activation, cotangent, (((0,), (0,)), ((...]
    all_gather x2 -> x1, blocking collectives: 49.2 us -> 5.42 us  [shards(): small_sum = jnp.sum(lax.all_gather(small_part, 'dp'), axis=0)]
    reduce_sum x3 -> x6, other arithmetic: 23.4 us -> 61.9 us  [the longest x2 29.8 us: shards(): jnp.sum(grad_conv * extended[begin:begin + row_count], axis=0)]
    broadcast_in_dim x1, other arithmetic: 18 us -> 48.2 us  [shards(): grad_gates[None]]
    unnamed x1 -> x0, blocking collectives: 20.8 us -> none
    ppermute x0 -> x14, waiting for transfers between devices: none -> 20.7 us  [the longest x6 14.4 us: bit_swap(): return lax.ppermute(value, axis, [(i, i ^ 1 << bit) for i in range(count)])]
    all_to_all x0 -> x1, starting transfers between devices: none -> 14.9 us  [shards(): small_part = lax.all_to_all(small_part, 'sp', 1, 0, tiled=True)]
    ppermute x0 -> x14, starting transfers between devices: none -> 14.4 us  [the longest x6 10.1 us: bit_swap(): return lax.ppermute(value, axis, [(i, i ^ 1 << bit) for i in range(count)])]
  transfers between devices with their start and end apart: 5 -> 17, of which waited for: 2 -> 5; matrix products, arithmetic and copies ran while one was open for 13% -> 71% of each run, Pallas kernels for 0% -> 0%
where the time goes in v1:
time: 235 us; the launch traced here: 234 us
  other arithmetic  125 us (53%)
  starting transfers between devices  33.9 us (14%)
  local copies, waits for them, and re-layouts  33.2 us (14%)
  waiting for transfers between devices  20.8 us (9%)
  matrix products  14.6 us (6%)
  blocking collectives  5.42 us (2%)
    broadcast_in_dim x1, other arithmetic, shards(): grad_gates[None]  48.2 us
    reduce_sum x2, other arithmetic, shards(): jnp.sum(grad_conv * extended[begin:begin + row_count], axis=0)  29.8 us
    reduce_sum x1, other arithmetic, shards(): centre = (jnp.sum(conv, axis=1) / width_float)[:, None]  28.8 us
    all_to_all x1, starting transfers between devices, shards(): small_part = lax.all_to_all(small_part, 'sp', 1, 0, tiled=True)  14.9 us
    ppermute x6, waiting for transfers between devices, bit_swap(): return lax.ppermute(value, axis, [(i, i ^ 1 << bit) for i in range(count)])  14.4 us
    ppermute x6, starting transfers between devices, bit_swap(): return lax.ppermute(value, axis, [(i, i ^ 1 << bit) for i in range(count)])  10.1 us
    unnamed x64, local copies, waits for them, and re-layouts  9.29 us
    ppermute x3, waiting for transfers between devices, chip_shift(): return lax.ppermute(value, 'dp', pairs)  6.35 us
  transfers between devices with their start and end apart: 17, of which 5 were waited for; matrix products, arithmetic and copies ran while one was open for 71% of the time, Pallas kernels for 0%

profile of v1, /device:TPU:0, one launch (start us, length us, event | category | flops | bytes accessed | tf_op | source)
XLA Modules:
  0.0 234.3 jit_solution(3892732511055882137)
XLA Ops:
  0.6 3.0 %collective-permute-start.4 = (bf16[256,2048]{1,0:T(8,128)(2,1)}, bf16[256,2048]{1,0:T(8,128)(2,1)}, u32[]{:S(2)}, u32[]{:S(2)}) collective-permute-start(bf16[256,2048]{1,0:T(8,128)(2,1)} %bitcast.239), channel_id=1, source_target_pairs={{0,2},{1,3},{2,0},{3,1},{4,6},{5,7},{6,4},{7,5},{8,10},{9,11},{10,... | collective-permute-start | bytes 3145736 | tf_op jit(solution)/shard_map/ppermute | solution.py:16
  5.6 1.5 collective-permute-start
  7.1 1.5 copy.47
  9.6 3.3 %collective-permute-start.6 = (bf16[30,2048]{0,1:T(8,128)(2,1)S(1)}, bf16[30,2048]{0,1:T(8,128)(2,1)}, u32[]{:S(2)}, u32[]{:S(2)}) collective-permute-start(bf16[30,2048]{0,1:T(8,128)(2,1)S(1)} %fusion.113), channel_id=1, source_target_pairs={{0,4},{4,8},{8,12},{12,16},{16,20},{20,24},{24,28},{1,5},{5,9},{9,... | collective-permute-start | bytes 368648 | tf_op jit(solution)/shard_map/ppermute | solution.py:31
  13.7 1.6 fusion.8
  15.3 1.5 collective-permute-done.1
  16.9 1.8 collective-permute-start.2
  18.7 2.7 %convolution_convert_fusion.3 = bf16[256,512]{1,0:T(8,128)(2,1)S(1)} fusion(bf16[512,2048]{1,0:T(8,128)(2,1)} %param.9, bf16[1,256,2048]{2,1,0:T(8,128)(2,1)} %param.6), kind=kOutput, calls=%fused_computation.214 | convolution fusion | flops 537001984 | bytes 3407872 | tf_op jit(solution)/shard_map/dot_general | solution.py:102
  21.5 1.3 collective-permute-done.2
  23.8 2.0 maximum_convert_fusion
  25.9 28.8 %fusion.118 = (f32[256]{0:T(256)S(1)}, f32[256]{0:T(256)S(1)}, f32[256,2048]{0,1:T(8,128)}) fusion(f32[286,2048]{0,1:T(8,128)S(1)} %maximum_convert_fusion, f32[2048]{0:T(1024)S(1)} %bitcast.144, f32[2048]{0:T(1024)S(1)} %bitcast.146, f32[2048]{0:T(1024)S(1)} %bitcast.148, f32[2048]{0:T(1024)S(1)} %bitcast.150, f32[2048]{0:T(1024)S(1)} %bitcast.152, ...), kind=kLoop, calls=%fused_computation.257 | loop fusion | flops 33553920 | bytes 67364864 | tf_op jit(solution)/shard_map/reduce_sum | solution.py:128
  55.3 2.7 %convolution_convert_fusion.1 = bf16[256,512]{1,0:T(8,128)(2,1)S(1)} fusion(bf16[256,2048]{1,0:T(8,128)(2,1)} %collective-permute-done.4, bf16[512,2048]{1,0:T(8,128)(2,1)} %param.9), kind=kOutput, calls=%fused_computation.212 | convolution fusion | flops 537001984 | bytes 3407872 | tf_op jit(solution)/shard_map/dot_general | solution.py:102
  58.0 2.7 %convolution_convert_fusion = bf16[256,512]{1,0:T(8,128)(2,1)S(1)} fusion(bf16[256,2048]{1,0:T(8,128)(2,1)} %collective-permute-done.4, bf16[512,2048]{1,0:T(8,128)(2,1)} %collective-permute-done.3), kind=kOutput, calls=%fused_computation.211 | convolution fusion | flops 537001984 | bytes 3407872 | tf_op jit(solution)/shard_map/dot_general | solution.py:103
  60.8 1.0 maximum_select_fusion.1
  61.8 2.3 convolution_convert_fusion.2
  64.1 0.9 maximum_select_fusion
  65.1 2.0 copy.44
  67.1 1.1 broadcast_in_dim.23
  68.2 1.9 constant_dynamic-update-slice_fusion.1
  70.1 6.3 %collective-permute-done.5 = bf16[256,1024]{1,0:T(8,128)(2,1)} collective-permute-done((bf16[256,1024]{1,0:T(8,128)(2,1)}, bf16[256,1024]{1,0:T(8,128)(2,1)}, u32[]{:S(2)}, u32[]{:S(2)}) %collective-permute-start.5) | collective-permute-done | bytes 524320 | tf_op jit(solution)/shard_map/ppermute | solution.py:16
  76.4 2.0 copy.45
  78.5 1.9 constant_dynamic-update-slice_fusion
  80.3 3.2 %multiply_reduce_fusion = (f32[2048]{0:T(1024)S(1)}, f32[256]{0:T(256)S(1)}, f32[256]{0:T(256)S(1)}, bf16[256,2048]{0,1:T(8,128)(2,1)S(1)}) fusion(f32[256,2048]{0,1:T(8,128)} %get-tuple-element.64, f32[256]{0:T(256)S(1)} %copy-done.27, f32[256]{0:T(256)S(1)} %copy-done.26, f32[2048]{0:T(1024)S(1)} %bitcast.204, ...), kind=kLoop, calls=%fused_computation.167 | loop fusion | flops 10483200 | bytes 4214784 | tf_op jit(solution)/shard_map/reduce_sum | solution.py:161
  85.6 17.4 %multiply_reduce_fusion.1 = (f32[2048]{0:T(1024)S(1)}, f32[2048]{0:T(1024)S(1)}, f32[2048]{0:T(1024)S(1)}, f32[2048]{0:T(1024)S(1)}, f32[2048]{0:T(1024)S(1)}, /...) fusion(f32[286,2048]{0,1:T(8,128)S(1)} %maximum_convert_fusion,, ...), kind=kLoop, calls=%fused_computation.168 | loop fusion | flops 27750400 | bytes 43151360 | tf_op jit(solution)/shard_map/reduce_sum | solution.py:173
  103.1 1.3 copy-done
  104.4 1.0 slice.559
  105.4 2.3 copy.50
  107.7 1.3 collective-permute-start.7
  109.0 1.9 constant_dynamic-slice_fusion
  111.4 12.4 %multiply_reduce_fusion.19 = (f32[2048]{0:T(1024)S(1)}, f32[2048]{0:T(1024)S(1)}, f32[2048]{0:T(1024)S(1)}, f32[2048]{0:T(1024)S(1)}, f32[2048]{0:T(1024)S(1)}, ...) fusion(f32[256,2048]{0,1:T(8,128)} %copy-done, ...), kind=kLoop, calls=%fused_computation.186 | loop fusion | flops 13604864 | bytes 29466624 | tf_op jit(solution)/shard_map/reduce_sum | solution.py:173
  123.8 3.0 %stack.131 = f32[32,8,256]{2,0,1:T(8,128)} concatenate(f32[1,8,256]{2,0,1:T(1,128)S(1)} %bitcast.237, f32[1,8,256]{2,0,1:T(1,128)S(1)} %bitcast.236, f32[1,8,256]{2,0,1:T(1,128)S(1)} %bitcast.235, f32[1,8,256]{2,0,1:T(1,128)S(1)} %bitcast.234, f32[1,8,256]{2,0,1:T(1,128)S(1)} %bitcast.233, f32[1,8,256]{2,0,1:T(1,128)S(1)} %bitcast.232, f32[1,8,256]{2,0,1:T(1,128)S(1)} %bitcast.231, ...), dimensions={0} | concatenate | bytes 524288 | tf_op jit(solution)/shard_map/stack | solution.py:174
  126.8 14.9 %all-to-all-start = ((f32[32,8,256]{2,0,1:T(8,128)}), f32[32,8,256]{2,0,1:T(8,128)S(1)}, u32[]{:S(2)}, u32[]{:S(2)}) async-start(f32[32,8,256]{2,0,1:T(8,128)} %stack.131), calls=%async_computation | async-start | bytes 524288 | tf_op jit(solution)/shard_map/all_to_all | solution.py:175
  141.7 2.3 copy.51
  144.0 4.2 %fusion = f32[4,2,64,2048]{3,2,1,0:T(8,128)S(1)} fusion(bf16[256,2048]{1,0:T(8,128)(2,1)} %collective-permute-done.12, bf16[256,2048]{1,0:T(8,128)(2,1)} %collective-permute-done.4, bf16[256,2048]{1,0:T(8,128)(2,1)} %collective-permute-done.11, bf16[256,2048]{1,0:T(8,128)(2,1)S(1)} %bitcast.241, bf16[4,2,64,256]{3,2,1,0:T(8,128)(2,1)} %bitcast.50, ...), kind=kOutput, calls=%fused_computation.59 | convolution fusion | flops 2168455168 | bytes 9437184 | tf_op jit(solution)/shard_map/dot_general | solution.py:155
  148.2 2.0 copy-done.8
  150.2 1.1 fusion.102
  151.4 2.0 collective-permute-start.13
  153.4 48.2 %fusion.103 = (bf16[1,256,2048]{1,2,0:T(8,128)(2,1)}, bf16[256,2048]{0,1:T(8,128)(2,1)}) fusion(bf16[1,256,2048]{1,2,0:T(8,128)(2,1)} %copy-done.5, bf16[1,256,2048]{1,2,0:T(8,128)(2,1)S(1)} %copy-done.3, f32[30,2048]{0,1:T(8,128)} %copy.51, f32[256,2048]{0,1:T(8,128)S(1)} %copy-done.1, f32[2048]{0:T(1024)S(1)} %bitcast.145, f32[2048]{0:T(1024)S(1)} %bitcast.147, ...), kind=kLoop, calls=%fused_computation.216 | loop fusion | flops 54001664 | bytes 6791168 | tf_op jit(solution)/shard_map/broadcast_in_dim | solution.py:188
  201.6 2.2 bitcast_add_fusion
  204.7 1.5 collective-permute-start.14
  206.2 1.7 fusion.104
  207.9 2.4 %copy.53 = bf16[1,256,2048]{2,1,0:T(8,128)(2,1)} copy(bf16[1,256,2048]{1,2,0:T(8,128)(2,1)} %fusion.104) | data formatting | bytes 2097152
  210.2 1.4 copy.54
  211.7 5.4 %all-gather = f32[128,256]{1,0:T(8,128)S(1)} all-gather(f32[32,256]{1,0:T(8,128)S(1)} %reduce_sum.378), channel_id=2, replica_groups=mesh['sp'=8,'dp'=4] {'dp'}, dimensions={0}, use_global_device_ids=true | all-gather | bytes 163840 | tf_op jit(solution)/shard_map/all_gather | solution.py:177
  217.1 0.9 collective-permute-done.14
  218.1 1.1 bitcast_add_fusion.1
  219.3 2.4 %collective-permute-start.15 = (bf16[1,64,2048]{2,1,0:T(8,128)(2,1)S(1)}, bf16[1,64,2048]{2,1,0:T(8,128)(2,1)S(1)}, u32[]{:S(2)}, u32[]{:S(2)}) collective-permute-start(bf16[1,64,2048]{2,1,0:T(8,128)(2,1)S(1)} %dynamic-slice_convert_fusion.1), channel_id=1, source_target_pairs={{0,16},{4,20},{8,24},{12,28},{16,0},{20,4},{24,8},{28,12},{1,17},{... | collective-permute-start | bytes 786440 | tf_op jit(solution)/shard_map/ppermute | solution.py:25
  222.9 10.6 %collective-permute-done.15 = bf16[1,64,2048]{2,1,0:T(8,128)(2,1)S(1)} collective-permute-done((bf16[1,64,2048]{2,1,0:T(8,128)(2,1)S(1)}, bf16[1,64,2048]{2,1,0:T(8,128)(2,1)S(1)}, u32[]{:S(2)}, u32[]{:S(2)}) %collective-permute-start.15) | collective-permute-done | bytes 262176 | tf_op jit(solution)/shard_map/ppermute | solution.py:25
  (100 shorter events, 10.8 us)
Async XLA Ops:
  0.6 7.9 %copy-start.9 = (bf16[1,256,2048]{2,1,0:T(8,128)(2,1)S(1)}, bf16[1,256,2048]{2,1,0:T(8,128)(2,1)}, u32[]{:S(2)}) copy-start(bf16[1,256,2048]{2,1,0:T(8,128)(2,1)} %param.7) | copy-start | bytes 3145732
  0.6 54.7 %collective-permute-start.4 = (bf16[256,2048]{1,0:T(8,128)(2,1)}, bf16[256,2048]{1,0:T(8,128)(2,1)}, u32[]{:S(2)}, u32[]{:S(2)}) collective-permute-start(bf16[256,2048]{1,0:T(8,128)(2,1)} %bitcast.239), channel_id=1, source_target_pairs={{0,2},{1,3},{2,0},{3,1},{4,6},{5,7},{6,4},{7,5},{8,10},{9,11},{10,... | collective-permute-start | bytes 3145736 | tf_op jit(solution)/shard_map/ppermute | solution.py:16
  3.7 140.3 %collective-permute-start.11 = (bf16[256,2048]{1,0:T(8,128)(2,1)}, bf16[256,2048]{1,0:T(8,128)(2,1)}, u32[]{:S(2)}, u32[]{:S(2)}) collective-permute-start(bf16[256,2048]{1,0:T(8,128)(2,1)} %bitcast.240), channel_id=1, source_target_pairs={{0,1},{1,0},{2,3},{3,2},{4,5},{5,4},{6,7},{7,6},{8,9},{9,8},{10,11... | collective-permute-start | bytes 3145736 | tf_op jit(solution)/shard_map/ppermute | solution.py:20
  3.7 54.4 %collective-permute-start.3 = (bf16[512,2048]{1,0:T(8,128)(2,1)}, bf16[512,2048]{1,0:T(8,128)(2,1)}, u32[]{:S(2)}, u32[]{:S(2)}) collective-permute-start(bf16[512,2048]{1,0:T(8,128)(2,1)} %param.9), channel_id=1, source_target_pairs={{0,1},{1,0},{2,3},{3,2},{4,5},{5,4},{6,7},{7,6},{8,9},{9,8},{10,11... | collective-permute-start | bytes 6291464 | tf_op jit(solution)/shard_map/ppermute | solution.py:20
  5.6 7.3 %collective-permute-start = (bf16[1,32,256]{2,1,0:T(8,128)(2,1)S(1)}, bf16[1,32,256]{2,1,0:T(8,128)(2,1)S(1)}, u32[]{:S(2)}, u32[]{:S(2)}) collective-permute-start(bf16[1,32,256]{2,1,0:T(8,128)(2,1)S(1)} %maximum_bitcast_fusion.2), channel_id=1, source_target_pairs={{0,4},{4,0},{8,12},{12,8},{16,20},{20,16},{24,28},{28,24},{1,5},{5... | collective-permute-start | bytes 49160 | tf_op jit(solution)/shard_map/ppermute | solution.py:25
  8.6 6.8 %copy-start.2 = (bf16[1,256,2048]{1,2,0:T(8,128)(2,1)}, bf16[1,256,2048]{1,2,0:T(8,128)(2,1)S(1)}, u32[]{:S(2)}) copy-start(bf16[1,256,2048]{1,2,0:T(8,128)(2,1)S(1)} %copy.47) | copy-start | bytes 3145732
  9.1 6.2 %copy-start.5 = (bf16[1,256,2048]{1,2,0:T(8,128)(2,1)}, bf16[1,256,2048]{1,2,0:T(8,128)(2,1)S(1)}, u32[]{:S(2)}) copy-start(bf16[1,256,2048]{1,2,0:T(8,128)(2,1)S(1)} %copy.46) | copy-start | bytes 3145732
  9.6 14.2 %collective-permute-start.6 = (bf16[30,2048]{0,1:T(8,128)(2,1)S(1)}, bf16[30,2048]{0,1:T(8,128)(2,1)}, u32[]{:S(2)}, u32[]{:S(2)}) collective-permute-start(bf16[30,2048]{0,1:T(8,128)(2,1)S(1)} %fusion.113), channel_id=1, source_target_pairs={{0,4},{4,8},{8,12},{12,16},{16,20},{20,24},{24,28},{1,5},{5,9},{9,... | collective-permute-start | bytes 368648 | tf_op jit(solution)/shard_map/ppermute | solution.py:31
  12.9 4.0 %collective-permute-start.1 = (bf16[2,32,256]{2,1,0:T(8,128)(2,1)S(1)}, bf16[2,32,256]{2,1,0:T(8,128)(2,1)S(1)}, u32[]{:S(2)}, u32[]{:S(2)}) collective-permute-start(bf16[2,32,256]{2,1,0:T(8,128)(2,1)S(1)} %maximum_select_fusion.4), channel_id=1, source_target_pairs={{0,8},{4,12},{8,0},{12,4},{16,24},{20,28},{24,16},{28,20},{1,9},{5... | collective-permute-start | bytes 98312 | tf_op jit(solution)/shard_map/ppermute | solution.py:25
  16.9 5.9 %collective-permute-start.2 = (bf16[4,32,256]{2,1,0:T(8,128)(2,1)S(1)}, bf16[4,32,256]{2,1,0:T(8,128)(2,1)S(1)}, u32[]{:S(2)}, u32[]{:S(2)}) collective-permute-start(bf16[4,32,256]{2,1,0:T(8,128)(2,1)S(1)} %maximum_select_fusion.3), channel_id=1, source_target_pairs={{0,16},{4,20},{8,24},{12,28},{16,0},{20,4},{24,8},{28,12},{1,17},{... | collective-permute-start | bytes 196616 | tf_op jit(solution)/shard_map/ppermute | solution.py:25
  23.0 2.8 %copy-start.12 = (f32[1,8,256]{2,0,1:T(1,128)}, f32[1,8,256]{2,0,1:T(1,128)S(1)}, u32[]{:S(2)}) copy-start(f32[1,8,256]{2,0,1:T(1,128)S(1)} %get-tuple-element.88) | copy-start | bytes 24580
  23.1 2.8 %copy-start.13 = (f32[1,8,256]{2,0,1:T(1,128)}, f32[1,8,256]{2,0,1:T(1,128)S(1)}, u32[]{:S(2)}) copy-start(f32[1,8,256]{2,0,1:T(1,128)S(1)} %get-tuple-element.89) | copy-start | bytes 24580
  23.1 2.8 %copy-start.14 = (f32[1,8,256]{2,0,1:T(1,128)}, f32[1,8,256]{2,0,1:T(1,128)S(1)}, u32[]{:S(2)}) copy-start(f32[1,8,256]{2,0,1:T(1,128)S(1)} %get-tuple-element.90) | copy-start | bytes 24580
  23.1 2.8 %copy-start.15 = (f32[1,8,256]{2,0,1:T(1,128)}, f32[1,8,256]{2,0,1:T(1,128)S(1)}, u32[]{:S(2)}) copy-start(f32[1,8,256]{2,0,1:T(1,128)S(1)} %get-tuple-element.91) | copy-start | bytes 24580
  23.1 2.8 %copy-start.16 = (f32[1,8,256]{2,0,1:T(1,128)}, f32[1,8,256]{2,0,1:T(1,128)S(1)}, u32[]{:S(2)}) copy-start(f32[1,8,256]{2,0,1:T(1,128)S(1)} %get-tuple-element.92) | copy-start | bytes 24580
  23.1 2.8 %copy-start.17 = (f32[1,8,256]{2,0,1:T(1,128)}, f32[1,8,256]{2,0,1:T(1,128)S(1)}, u32[]{:S(2)}) copy-start(f32[1,8,256]{2,0,1:T(1,128)S(1)} %get-tuple-element.93) | copy-start | bytes 24580
  23.1 2.8 %copy-start.18 = (f32[1,8,256]{2,0,1:T(1,128)}, f32[1,8,256]{2,0,1:T(1,128)S(1)}, u32[]{:S(2)}) copy-start(f32[1,8,256]{2,0,1:T(1,128)S(1)} %get-tuple-element.94) | copy-start | bytes 24580
  23.1 2.8 %copy-start.19 = (f32[1,8,256]{2,0,1:T(1,128)}, f32[1,8,256]{2,0,1:T(1,128)S(1)}, u32[]{:S(2)}) copy-start(f32[1,8,256]{2,0,1:T(1,128)S(1)} %get-tuple-element.95) | copy-start | bytes 24580
  23.1 2.8 %copy-start.20 = (f32[1,8,256]{2,0,1:T(1,128)}, f32[1,8,256]{2,0,1:T(1,128)S(1)}, u32[]{:S(2)}) copy-start(f32[1,8,256]{2,0,1:T(1,128)S(1)} %get-tuple-element.96) | copy-start | bytes 24580
  23.1 2.8 %copy-start.21 = (f32[1,8,256]{2,0,1:T(1,128)}, f32[1,8,256]{2,0,1:T(1,128)S(1)}, u32[]{:S(2)}) copy-start(f32[1,8,256]{2,0,1:T(1,128)S(1)} %get-tuple-element.97) | copy-start | bytes 24580
  23.1 2.8 %copy-start.22 = (f32[1,8,256]{2,0,1:T(1,128)}, f32[1,8,256]{2,0,1:T(1,128)S(1)}, u32[]{:S(2)}) copy-start(f32[1,8,256]{2,0,1:T(1,128)S(1)} %get-tuple-element.98) | copy-start | bytes 24580
  23.2 2.8 %copy-start.23 = (f32[1,8,256]{2,0,1:T(1,128)}, f32[1,8,256]{2,0,1:T(1,128)S(1)}, u32[]{:S(2)}) copy-start(f32[1,8,256]{2,0,1:T(1,128)S(1)} %get-tuple-element.99) | copy-start | bytes 24580
  23.2 2.8 %copy-start.24 = (f32[1,8,256]{2,0,1:T(1,128)}, f32[1,8,256]{2,0,1:T(1,128)S(1)}, u32[]{:S(2)}) copy-start(f32[1,8,256]{2,0,1:T(1,128)S(1)} %get-tuple-element.100) | copy-start | bytes 24580
  55.3 88.6 %collective-permute-start.12 = (bf16[256,2048]{1,0:T(8,128)(2,1)}, bf16[256,2048]{1,0:T(8,128)(2,1)}, u32[]{:S(2)}, u32[]{:S(2)}) collective-permute-start(bf16[256,2048]{1,0:T(8,128)(2,1)} %collective-permute-done.4), channel_id=1, source_target_pairs={{0,1},{1,0},{2,3},{3,2},{4,5},{5,4},{6,7},{7,6},{8,9},{9,8},{10,11... | collective-permute-start | bytes 3145736 | tf_op jit(solution)/shard_map/ppermute | solution.py:20
  58.0 3.8 %copy-start.28 = (bf16[1,256,2048]{2,1,0:T(8,128)(2,1)S(1)}, bf16[1,256,2048]{2,1,0:T(8,128)(2,1)}, u32[]{:S(2)}) copy-start(bf16[1,256,2048]{2,1,0:T(8,128)(2,1)} %param.6) | copy-start | bytes 3145732
  61.8 14.6 %collective-permute-start.5 = (bf16[256,1024]{1,0:T(8,128)(2,1)}, bf16[256,1024]{1,0:T(8,128)(2,1)}, u32[]{:S(2)}, u32[]{:S(2)}) collective-permute-start(bf16[256,1024]{1,0:T(8,128)(2,1)} %maximum_select_fusion.1), channel_id=1, source_target_pairs={{0,2},{1,3},{2,0},{3,1},{4,6},{5,7},{6,4},{7,5},{8,10},{9,11},{10,... | collective-permute-start | bytes 1572872 | tf_op jit(solution)/shard_map/ppermute | solution.py:16
  67.1 13.2 %copy-start.25 = (f32[1,8,256]{2,0,1:T(1,128)S(1)}, f32[1,8,256]{2,0,1:T(1,128)}, u32[]{:S(2)}) copy-start(f32[1,8,256]{2,0,1:T(1,128)} %slice_convert_fusion.1) | copy-start | bytes 24580
  67.1 13.2 %copy-start.26 = (f32[256]{0:T(256)S(1)}, f32[256]{0:T(256)}, u32[]{:S(2)}) copy-start(f32[256]{0:T(256)} %get-tuple-element.101) | copy-start | bytes 3076
  67.1 13.2 %copy-start.27 = (f32[256]{0:T(256)S(1)}, f32[256]{0:T(256)}, u32[]{:S(2)}) copy-start(f32[256]{0:T(256)} %get-tuple-element.102) | copy-start | bytes 3076
  83.6 2.0 copy-start.4
  84.4 24.6 %collective-permute-start.9 = (bf16[8,2,64,256]{3,2,1,0:T(8,128)(2,1)}, bf16[8,2,64,256]{3,2,1,0:T(8,128)(2,1)}, u32[]{:S(2)}, u32[]{:S(2)}) collective-permute-start(bf16[8,2,64,256]{3,2,1,0:T(8,128)(2,1)} %dynamic-slice_bitcast_fusion), channel_id=1, source_target_pairs={{0,2},{1,3},{2,0},{3,1},{4,6},{5,7},{6,4},{7,5},{8,10},{9,11},{10,... | collective-permute-start | bytes 1572872 | tf_op jit(solution)/shard_map/ppermute | solution.py:16
  85.6 58.4 %collective-permute-start.8 = (bf16[8,64,256]{2,1,0:T(8,128)(2,1)}, bf16[8,64,256]{2,1,0:T(8,128)(2,1)}, u32[]{:S(2)}, u32[]{:S(2)}) collective-permute-start(bf16[8,64,256]{2,1,0:T(8,128)(2,1)} %get-tuple-element.67), channel_id=1, source_target_pairs={{0,1},{1,0},{2,3},{3,2},{4,5},{5,4},{6,7},{7,6},{8,9},{9,8},{10,11... | collective-permute-start | bytes 786440 | tf_op jit(solution)/shard_map/ppermute | solution.py:20
  103.0 1.4 copy-start
  107.7 34.0 %collective-permute-start.7 = (f32[30,2048]{1,0:T(8,128)}, f32[30,2048]{1,0:T(8,128)}, u32[]{:S(2)}, u32[]{:S(2)}) collective-permute-start(f32[30,2048]{1,0:T(8,128)} %copy.50), channel_id=1, source_target_pairs={{4,0},{8,4},{12,8},{16,12},{20,16},{24,20},{28,24},{5,1},{9,5},{13... | collective-permute-start | bytes 737288 | tf_op jit(solution)/shard_map/ppermute | solution.py:31
  110.9 33.1 %collective-permute-start.10 = (bf16[8,64,256]{2,1,0:T(8,128)(2,1)}, bf16[8,64,256]{2,1,0:T(8,128)(2,1)}, u32[]{:S(2)}, u32[]{:S(2)}) collective-permute-start(bf16[8,64,256]{2,1,0:T(8,128)(2,1)} %get-tuple-element.69), channel_id=1, source_target_pairs={{0,1},{1,0},{2,3},{3,2},{4,5},{5,4},{6,7},{7,6},{8,9},{9,8},{10,11... | collective-permute-start | bytes 786440 | tf_op jit(solution)/shard_map/ppermute | solution.py:20
  123.8 20.2 %copy-start.10 = (bf16[8,1,1,64,256]{4,3,2,1,0:T(8,128)(2,1)S(1)}, bf16[8,1,1,64,256]{4,3,2,1,0:T(8,128)(2,1)}, u32[]{:S(2)}) copy-start(bf16[8,1,1,64,256]{4,3,2,1,0:T(8,128)(2,1)} %get-tuple-element.66) | copy-start | bytes 786436
  123.8 20.2 %copy-start.11 = (bf16[8,1,64,256]{3,2,1,0:T(8,128)(2,1)S(1)}, bf16[8,1,64,256]{3,2,1,0:T(8,128)(2,1)}, u32[]{:S(2)}) copy-start(bf16[8,1,64,256]{3,2,1,0:T(8,128)(2,1)} %get-tuple-element.68) | copy-start | bytes 786436
  123.8 20.2 %copy-start.29 = (bf16[1,256,2048]{2,1,0:T(8,128)(2,1)S(1)}, bf16[1,256,2048]{2,1,0:T(8,128)(2,1)}, u32[]{:S(2)}) copy-start(bf16[1,256,2048]{2,1,0:T(8,128)(2,1)} %param.6) | copy-start | bytes 3145732
  126.8 84.9 %all-to-all-start = ((f32[32,8,256]{2,0,1:T(8,128)}), f32[32,8,256]{2,0,1:T(8,128)S(1)}, u32[]{:S(2)}, u32[]{:S(2)}) async-start(f32[32,8,256]{2,0,1:T(8,128)} %stack.131), calls=%async_computation | async-start | bytes 524288 | tf_op jit(solution)/shard_map/all_to_all | solution.py:175
  144.0 9.4 %copy-start.3 = (bf16[1,256,2048]{1,2,0:T(8,128)(2,1)S(1)}, bf16[1,256,2048]{1,2,0:T(8,128)(2,1)}, u32[]{:S(2)}) copy-start(bf16[1,256,2048]{1,2,0:T(8,128)(2,1)} %copy-done.2) | copy-start | bytes 3145732
  148.2 2.1 copy-start.8
  150.2 3.2 %copy-start.1 = (f32[256,2048]{0,1:T(8,128)S(1)}, f32[256,2048]{0,1:T(8,128)}, u32[]{:S(2)}) copy-start(f32[256,2048]{0,1:T(8,128)} %copy-done) | copy-start | bytes 6291460
  151.4 50.2 %collective-permute-start.13 = (bf16[4,64,2048]{2,1,0:T(8,128)(2,1)}, bf16[4,64,2048]{2,1,0:T(8,128)(2,1)}, u32[]{:S(2)}, u32[]{:S(2)}) collective-permute-start(bf16[4,64,2048]{2,1,0:T(8,128)(2,1)} %fusion.102), channel_id=1, source_target_pairs={{0,4},{4,0},{8,12},{12,8},{16,20},{20,16},{24,28},{28,24},{1,5},{5... | collective-permute-start | bytes 3145736 | tf_op jit(solution)/shard_map/ppermute | solution.py:25
  201.6 4.6 %copy-start.6 = (bf16[256,2048]{0,1:T(8,128)(2,1)S(1)}, bf16[256,2048]{0,1:T(8,128)(2,1)}, u32[]{:S(2)}) copy-start(bf16[256,2048]{0,1:T(8,128)(2,1)} %get-tuple-element.63) | copy-start | bytes 3145732
  204.7 13.3 %collective-permute-start.14 = (bf16[2,64,2048]{2,1,0:T(8,128)(2,1)}, bf16[2,64,2048]{2,1,0:T(8,128)(2,1)}, u32[]{:S(2)}, u32[]{:S(2)}) collective-permute-start(bf16[2,64,2048]{2,1,0:T(8,128)(2,1)} %fusion.112), channel_id=1, source_target_pairs={{0,8},{4,12},{8,0},{12,4},{16,24},{20,28},{24,16},{28,20},{1,9},{5... | collective-permute-start | bytes 1572872 | tf_op jit(solution)/shard_map/ppermute | solution.py:25
  207.9 2.4 %copy-start.7 = (bf16[1,256,2048]{1,2,0:T(8,128)(2,1)S(1)}, bf16[1,256,2048]{1,2,0:T(8,128)(2,1)}, u32[]{:S(2)}) copy-start(bf16[1,256,2048]{1,2,0:T(8,128)(2,1)} %get-tuple-element.62) | copy-start | bytes 3145732
  219.3 14.2 %collective-permute-start.15 = (bf16[1,64,2048]{2,1,0:T(8,128)(2,1)S(1)}, bf16[1,64,2048]{2,1,0:T(8,128)(2,1)S(1)}, u32[]{:S(2)}, u32[]{:S(2)}) collective-permute-start(bf16[1,64,2048]{2,1,0:T(8,128)(2,1)S(1)} %dynamic-slice_convert_fusion.1), channel_id=1, source_target_pairs={{0,16},{4,20},{8,24},{12,28},{16,0},{20,4},{24,8},{28,12},{1,17},{... | collective-permute-start | bytes 786440 | tf_op jit(solution)/shard_map/ppermute | solution.py:25

commit v2 on v1

v2 whole, which is shorter than its diff:
```python
import functools

import jax
import jax.numpy as jnp
from jax import lax
from jax.experimental import pallas as pl
from jax.experimental.pallas import tpu as pltpu
from jax.sharding import PartitionSpec as P

epsilon = 1e-05
CORES = 2
LANES = 128
PAD = 32


def sigmoid(value):
    return 1.0 / (1.0 + jnp.exp(-value))


def forward_body(taps_count, value, gate, front, taps, act, centred, gated, inv, held, conv):
    rows, width = value.shape
    columns = width // LANES
    step = pl.program_id(0)

    @pl.when(step == 0)
    def _():
        for c in range(columns):
            held[c, :PAD, :] = front[:, c * LANES : (c + 1) * LANES].astype(jnp.float32)

    @pl.when(step > 0)
    def _():
        for c in range(columns):
            held[c, :PAD, :] = held[c, rows : rows + PAD, :]

    def convolve(c, total):
        lanes = pl.ds(pl.multiple_of(c * LANES, LANES), LANES)
        product = value[:, lanes].astype(jnp.float32) * sigmoid(gate[:, lanes].astype(jnp.float32))
        product = product.astype(jnp.bfloat16)
        gated[:, lanes] = product
        held[c, PAD : PAD + rows, :] = product.astype(jnp.float32)
        result = jnp.zeros((rows, LANES), jnp.float32)
        for k in range(taps_count):
            result = result + taps[c, k : k + 1, :] * held[c, PAD - k : PAD - k + rows, :]
        conv[c] = result
        return total + result

    zeros = jnp.zeros((rows, LANES), jnp.float32)
    total = lax.fori_loop(0, columns, convolve, zeros)
    centre = jnp.sum(total, axis=1, keepdims=True) * (1.0 / width)

    def squares(c, total):
        off = conv[c] - centre
        conv[c] = off
        return total + off * off

    total = lax.fori_loop(0, columns, squares, zeros)
    variance = jnp.sum(total, axis=1, keepdims=True) * (1.0 / width)
    scale = lax.rsqrt(variance + epsilon)
    inv[...] = jnp.broadcast_to(scale, inv.shape)

    def normalize(c, carry):
        lanes = pl.ds(pl.multiple_of(c * LANES, LANES), LANES)
        value_c = conv[c] * scale
        centred[c] = value_c
        normed = value_c * taps[c, taps_count : taps_count + 1, :]
        act[:, lanes] = (normed * sigmoid(normed)).astype(jnp.bfloat16)
        return carry

    lax.fori_loop(0, columns, normalize, 0)


def forward(values_in, gates_in, front, taps, taps_count):
    rows, width = values_in.shape
    columns = width // LANES
    block = 64
    by_rows = pl.BlockSpec((block, width), lambda i: (i, 0))
    return pl.pallas_call(
        functools.partial(forward_body, taps_count),
        grid=(rows // block,),
        in_specs=[
            by_rows,
            by_rows,
            pl.BlockSpec((PAD, width), lambda i: (0, 0)),
            pl.BlockSpec(taps.shape, lambda i: (0, 0, 0)),
        ],
        out_specs=[
            by_rows,
            pl.BlockSpec((columns, block, LANES), lambda i: (0, i, 0)),
            by_rows,
            pl.BlockSpec((block, LANES), lambda i: (i, 0)),
        ],
        out_shape=[
            jax.ShapeDtypeStruct((rows, width), jnp.bfloat16),
            jax.ShapeDtypeStruct((columns, rows, LANES), jnp.float32),
            jax.ShapeDtypeStruct((rows, width), jnp.bfloat16),
            jax.ShapeDtypeStruct((rows, LANES), jnp.float32),
        ],
        scratch_shapes=[
            pltpu.VMEM((columns, PAD + block, LANES), jnp.float32),
            pltpu.VMEM((columns, block, LANES), jnp.float32),
        ],
        cost_estimate=pl.CostEstimate(
            flops=rows * width * 100, bytes_accessed=rows * width * 12, transcendentals=0
        ),
        name="forward",
    )(values_in, gates_in, front, taps)


def normed_back_body(taps_count, grad_act, centred, inv, taps, grad_conv, gain_part, held):
    rows, width = grad_act.shape
    columns = width // LANES

    @pl.when(pl.program_id(0) == 0)
    def _():
        gain_part[...] = jnp.zeros(gain_part.shape, jnp.float32)

    def products(c, totals):
        lanes = pl.ds(pl.multiple_of(c * LANES, LANES), LANES)
        gain = taps[c, taps_count : taps_count + 1, :]
        centred_c = centred[c]
        normed = centred_c * gain
        sig = sigmoid(normed)
        grad_normed = grad_act[:, lanes].astype(jnp.float32) * sig * (1.0 + normed * (1.0 - sig))
        part = (grad_normed * centred_c).reshape(rows // 8, 8, LANES)
        gain_part[:, lanes] += jnp.sum(part, axis=0)
        grad_centred = grad_normed * gain
        held[c] = grad_centred
        return (totals[0] + grad_centred, totals[1] + grad_centred * centred_c)

    zeros = jnp.zeros((rows, LANES), jnp.float32)
    first, second = lax.fori_loop(0, columns, products, (zeros, zeros))
    first = jnp.sum(first, axis=1, keepdims=True) * (1.0 / width)
    second = jnp.sum(second, axis=1, keepdims=True) * (1.0 / width)
    scale = inv[...]

    def finish(c, carry):
        grad_conv[c] = (held[c] - first - centred[c] * second) * scale
        return carry

    lax.fori_loop(0, columns, finish, 0)


def normed_back(grad_act, centred, inv, taps, taps_count):
    rows, width = grad_act.shape
    columns = width // LANES
    block = 64
    by_columns = pl.BlockSpec((columns, block, LANES), lambda i: (0, i, 0))
    return pl.pallas_call(
        functools.partial(normed_back_body, taps_count),
        grid=(rows // block,),
        in_specs=[
            pl.BlockSpec((block, width), lambda i: (i, 0)),
            by_columns,
            pl.BlockSpec((block, LANES), lambda i: (i, 0)),
            pl.BlockSpec(taps.shape, lambda i: (0, 0, 0)),
        ],
        out_specs=[by_columns, pl.BlockSpec((8, width), lambda i: (0, 0))],
        out_shape=[
            jax.ShapeDtypeStruct((columns, rows, LANES), jnp.float32),
            jax.ShapeDtypeStruct((8, width), jnp.float32),
        ],
        scratch_shapes=[pltpu.VMEM((columns, block, LANES), jnp.float32)],
        cost_estimate=pl.CostEstimate(
            flops=rows * width * 40, bytes_accessed=rows * width * 10, transcendentals=0
        ),
        name="normed_back",
    )(grad_act, centred, inv, taps)


def taps_back_body(taps_count, grad_conv, gated, front, gain_part, out, held):
    rows = gated.shape[0]
    held[:PAD, :] = front[...].astype(jnp.float32)
    held[PAD:, :] = gated[...].astype(jnp.float32)
    sums = [jnp.zeros((8, LANES), jnp.float32) for _ in range(taps_count)]
    for j in range(0, rows, 8):
        grad = grad_conv[0, j : j + 8, :]
        for k in range(taps_count):
            begin = j + PAD - k
            sums[k] = sums[k] + grad * held[begin : begin + 8, :]
    for k in range(taps_count):
        out[k : k + 1, :] = jnp.sum(sums[k], axis=0, keepdims=True)
    out[taps_count : taps_count + 1, :] = jnp.sum(gain_part[...], axis=0, keepdims=True)


def taps_back(grad_conv, gated, front, gain_part, taps_count):
    columns, rows, _ = grad_conv.shape
    width = columns * LANES
    return pl.pallas_call(
        functools.partial(taps_back_body, taps_count),
        grid=(columns,),
        in_specs=[
            pl.BlockSpec((1, rows, LANES), lambda c: (c, 0, 0)),
            pl.BlockSpec((rows, LANES), lambda c: (0, c)),
            pl.BlockSpec((PAD, LANES), lambda c: (0, c)),
            pl.BlockSpec((8, LANES), lambda c: (0, c)),
        ],
        out_specs=pl.BlockSpec((taps_count + 1, LANES), lambda c: (0, c)),
        out_shape=jax.ShapeDtypeStruct((taps_count + 1, width), jnp.float32),
        scratch_shapes=[pltpu.VMEM((PAD + rows, LANES), jnp.float32)],
        cost_estimate=pl.CostEstimate(
            flops=rows * width * 62, bytes_accessed=rows * width * 6, transcendentals=0
        ),
        name="taps_back",
    )(grad_conv, gated, front, gain_part)


def gated_back_body(taps_count, grad_conv, after, taps, value, gate, grad_value, grad_gate, held):
    rows = value.shape[0]
    block = 64
    held[:rows, :] = grad_conv[0]
    held[rows:, :] = after[0]
    for begin in range(0, rows, block):
        result = jnp.zeros((block, LANES), jnp.float32)
        for k in range(taps_count):
            result = result + taps[0, k : k + 1, :] * held[begin + k : begin + k + block, :]
        result = result.astype(jnp.bfloat16).astype(jnp.float32)
        sig = sigmoid(gate[begin : begin + block, :].astype(jnp.float32))
        grad_sig = result * sig
        grad_value[begin : begin + block, :] = grad_sig.astype(jnp.bfloat16)
        grad_gate[begin : begin + block, :] = (
            grad_sig * value[begin : begin + block, :].astype(jnp.float32) * (1.0 - sig)
        ).astype(jnp.bfloat16)


def gated_back(grad_conv, after, taps, values_in, gates_in, taps_count):
    columns, rows, _ = grad_conv.shape
    width = columns * LANES
    flat = pl.BlockSpec((rows, LANES), lambda c: (0, c))
    return pl.pallas_call(
        functools.partial(gated_back_body, taps_count),
        grid=(columns,),
        in_specs=[
            pl.BlockSpec((1, rows, LANES), lambda c: (c, 0, 0)),
            pl.BlockSpec((1, PAD, LANES), lambda c: (c, 0, 0)),
            pl.BlockSpec((1,) + taps.shape[1:], lambda c: (c, 0, 0)),
            flat,
            flat,
        ],
        out_specs=[flat, flat],
        out_shape=[jax.ShapeDtypeStruct((rows, width), jnp.bfloat16)] * 2,
        scratch_shapes=[pltpu.VMEM((PAD + rows, LANES), jnp.float32)],
        cost_estimate=pl.CostEstimate(
            flops=rows * width * 75, bytes_accessed=rows * width * 12, transcendentals=0
        ),
        name="gated_back",
    )(grad_conv, after, taps, values_in, gates_in)


def chip_shift(value, chips, cores, steps):
    pairs = [
        (chip * cores + core, (chip + steps) % chips * cores + core)
        for chip in range(chips)
        for core in range(cores)
    ]
    return lax.ppermute(value, "dp", pairs)


def core_swap(value, chips, cores):
    return lax.ppermute(value, "dp", [(i, i ^ 1) for i in range(chips * cores)])


def bit_swap(value, axis, bit):
    count = lax.axis_size(axis)
    return lax.ppermute(value, axis, [(i, i ^ (1 << bit)) for i in range(count)])


def passed_along(value, axis, steps):
    count = lax.axis_size(axis)
    initial, last = (max(0, -steps), min(count, count - steps))
    return lax.ppermute(value, axis, [(source, source + steps) for source in range(initial, last)])


def gathered(value, axis):
    count = lax.axis_size(axis)
    bits = count.bit_length() - 1
    me = lax.axis_index(axis)
    whole = value[None]
    for bit in range(bits):
        other = bit_swap(whole, axis, bit)
        mine_first = ((me >> bit) & 1) == 0
        whole = jnp.where(
            mine_first,
            jnp.concatenate([whole, other], axis=0),
            jnp.concatenate([other, whole], axis=0),
        )
    return whole


def gated_forward(values_in, gates_in):
    return (values_in.astype(jnp.float32) * jax.nn.sigmoid(gates_in.astype(jnp.float32))).astype(
        jnp.bfloat16
    )


def scattered_sum(parts, axis):
    count = lax.axis_size(axis)
    bits = count.bit_length() - 1
    me = lax.axis_index(axis)
    for bit in range(bits):
        mine = (me >> bit) & 1
        pairs = parts.reshape((parts.shape[0] // 2, 2) + parts.shape[1:])
        keep = lax.dynamic_index_in_dim(pairs, mine, axis=1, keepdims=False)
        send = lax.dynamic_index_in_dim(pairs, 1 - mine, axis=1, keepdims=False)
        parts = keep + bit_swap(send.astype(jnp.bfloat16), axis, bit).astype(jnp.float32)
    return parts[0]


def shards(out_cotangent, value_pre, gate_pre, out_weight, conv_kernel, norm_gain):
    cotangent = out_cotangent[0]
    values_in = value_pre[0]
    gates_in = gate_pre[0]
    row_count, width = cotangent.shape
    taps_count = conv_kernel.shape[0]
    sp_count, dp_count = lax.axis_size("sp"), lax.axis_size("dp")
    cores = CORES if dp_count % CORES == 0 else 1
    chips = dp_count // cores
    place = lax.axis_index("dp")
    chip, core = place // cores, place % cores

    small = gathered(jnp.concatenate([conv_kernel, norm_gain[None]], axis=0), "sp")
    front = passed_along(
        gated_forward(values_in[row_count - PAD :], gates_in[row_count - PAD :]), "sp", 1
    )
    cots = [cotangent] + [chip_shift(cotangent, chips, cores, k) for k in range(1, chips)]
    weight_other = core_swap(out_weight, chips, cores) if cores > 1 else None

    def times_weights(cot):
        dims = (((1,), (1,)), ((), ()))
        mine = lax.dot_general(cot, out_weight, dims, preferred_element_type=jnp.float32)
        mine = mine.astype(jnp.bfloat16)
        if cores == 1:
            return mine
        other = lax.dot_general(cot, weight_other, dims, preferred_element_type=jnp.float32)
        other = other.astype(jnp.bfloat16)
        return jnp.where(
            core == 0,
            jnp.concatenate([mine, other], axis=1),
            jnp.concatenate([other, mine], axis=1),
        )

    taps = small.astype(jnp.float32)
    taps = taps.reshape(width // LANES if taps.shape[2] == LANES else sp_count, taps_count + 1, -1)
    if taps.shape[2] != LANES:
        taps = taps.reshape(sp_count, taps_count + 1, -1, LANES).transpose(0, 2, 1, 3)
        taps = taps.reshape(-1, taps_count + 1, LANES)
    activation, centred, gated, inv = forward(values_in, gates_in, front, taps, taps_count)

    grad_act = jnp.zeros((row_count, width), jnp.bfloat16)
    for k in range(chips):
        piece = times_weights(cots[k])
        if k:
            piece = chip_shift(piece, chips, cores, -k)
        grad_act = lax.dynamic_update_slice(
            grad_act, piece, (0, (chip + k) % chips * piece.shape[1])
        )

    rows_out = width // (sp_count * dp_count)
    act_parts = activation.reshape(row_count, sp_count, chips, cores * rows_out)

    def for_chip(k):
        part = lax.dynamic_index_in_dim(act_parts, (chip + k) % chips, axis=2, keepdims=False)
        return part.reshape(row_count, -1)

    acts = [for_chip(0)] + [
        chip_shift(for_chip(k), chips, cores, k) for k in range(1, chips)
    ]
    weight_part = sum(
        lax.dot_general(act, cot, (((0,), (0,)), ((), ())), preferred_element_type=jnp.float32)
        for act, cot in zip(acts, cots)
    )
    weight_part = weight_part.reshape(sp_count, cores, rows_out, width)
    if cores > 1:
        keep = lax.dynamic_index_in_dim(weight_part, core, axis=1, keepdims=False)
        send = lax.dynamic_index_in_dim(weight_part, 1 - core, axis=1, keepdims=False)
        send = core_swap(send.astype(jnp.bfloat16), chips, cores)
        weight_part = keep + send.astype(jnp.float32)
    else:
        weight_part = weight_part[:, 0]
    weight_sum = scattered_sum(weight_part, "sp")

    grad_conv, gain_part = normed_back(grad_act, centred, inv, taps, taps_count)
    after = passed_along(grad_conv[:, :PAD], "sp", -1)
    small_part = taps_back(grad_conv, gated, front, gain_part, taps_count)
    small_part = lax.all_to_all(small_part, "sp", 1, 0, tiled=True)
    small_part = jnp.sum(small_part.reshape(sp_count, taps_count + 1, -1), axis=0)
    small_sum = jnp.sum(lax.all_gather(small_part, "dp"), axis=0)
    grad_values, grad_gates = gated_back(grad_conv, after, taps, values_in, gates_in, taps_count)

    factor = float(sp_count * dp_count * row_count) ** (-0.5)
    return (
        grad_values[None],
        grad_gates[None],
        weight_sum * factor,
        small_sum[:taps_count] * factor,
        small_sum[taps_count] * factor,
    )


def solution(mesh):
    placed = (
        P("dp", "sp", None),
        P("dp", "sp", None),
        P("dp", "sp", None),
        P("dp", None),
        P(None, "sp"),
        P("sp"),
    )
    return jax.shard_map(
        shards,
        mesh=mesh,
        in_specs=placed,
        out_specs=(
            P("dp", "sp", None),
            P("dp", "sp", None),
            P(("sp", "dp"), None),
            P(None, "sp"),
            P("sp"),
        ),
        check_vma=False,
    )
```

time: 235 us -> 166 us (0.71)
  other arithmetic: 125 us -> 9.75 us
  Pallas kernels: 0 us -> 41.2 us
  waiting for transfers between devices: 20.8 us -> 48.1 us
  local copies, waits for them, and re-layouts: 33.2 us -> 17.6 us
  starting transfers between devices: 33.9 us -> 27 us
    reduce_sum x4 -> x0, other arithmetic: 61.8 us -> none  [the longest x2 29.8 us: shards(): jnp.sum(grad_conv * extended[begin:begin + row_count], axis=0)]
    broadcast_in_dim x2 -> x0, other arithmetic: 49.9 us -> none  [the longest x1 48.2 us: shards(): grad_gates[None]]
    pallas_call x0 -> x4, Pallas kernels: none -> 41.2 us  [the longest x1 12.3 us: gated_back(): pl.pallas_call(functools.partial(gated_back_body, taps_count), grid=(colu...]
    ppermute x6, waiting for transfers between devices: 14.4 us -> 29.2 us  [bit_swap(): return lax.ppermute(value, axis, [(i, i ^ 1 << bit) for i in range(count)])]
    all_to_all x1, starting transfers between devices: 14.9 us -> 3.41 us  [shards(): small_part = lax.all_to_all(small_part, 'sp', 1, 0, tiled=True)]
    ppermute x2, waiting for transfers between devices: 0.01 us -> 9.37 us  [passed_along(): lax.ppermute(value, axis, [(source, source + steps) for source in range(i...]
    ppermute x2 -> x0, local copies, waits for them, and re-layouts: 4.31 us -> none  [the longest x1 2.27 us: passed_along(): lax.ppermute(value, axis, [(source, source + steps) for source in range(i...]
    dynamic_update_slice x2 -> x1, local copies, waits for them, and re-layouts: 3.76 us -> 0.04 us  [shards(): lax.dynamic_update_slice(grad_act, piece, (0, (chip + k) % chips * piece....]
  transfers between devices with their start and end apart: 17 -> 14, of which waited for: 5 -> 8; matrix products, arithmetic and copies ran while one was open for 71% -> 18% of each run, Pallas kernels for 0% -> 25%
where the time goes in v2:
time: 166 us; the launch traced here: 165 us
  waiting for transfers between devices  48.1 us (29%)
  Pallas kernels  41.2 us (25%)
  starting transfers between devices  27 us (16%)
  local copies, waits for them, and re-layouts  17.6 us (11%)
  matrix products  15 us (9%)
  other arithmetic  9.75 us (6%)
  blocking collectives  5.42 us (3%)
    ppermute x6, waiting for transfers between devices, bit_swap(): return lax.ppermute(value, axis, [(i, i ^ 1 << bit) for i in range(count)])  29.2 us
    ppermute x6, starting transfers between devices, bit_swap(): return lax.ppermute(value, axis, [(i, i ^ 1 << bit) for i in range(count)])  13.7 us
    pallas_call x1, Pallas kernels, gated_back(): pl.pallas_call(functools.partial(gated_back_body, taps_count), grid=(colu...  12.3 us
    pallas_call x1, Pallas kernels, taps_back(): pl.pallas_call(functools.partial(taps_back_body, taps_count), grid=(colum...  12.1 us
    pallas_call x1, Pallas kernels, forward(): pl.pallas_call(functools.partial(forward_body, taps_count), grid=(rows //...  11.1 us
    ppermute x2, waiting for transfers between devices, passed_along(): lax.ppermute(value, axis, [(source, source + steps) for source in range(i...  9.37 us
    unnamed x12, local copies, waits for them, and re-layouts  8.76 us
    ppermute x3, waiting for transfers between devices, chip_shift(): return lax.ppermute(value, 'dp', pairs)  8.41 us
  transfers between devices with their start and end apart: 14, of which 8 were waited for; matrix products, arithmetic and copies ran while one was open for 18% of the time, Pallas kernels for 25%

profile of v2, /device:TPU:0, one launch (start us, length us, event | category | flops | bytes accessed | tf_op | source)
XLA Modules:
  0.0 164.9 jit_solution(7029783701829365424)
XLA Ops:
  0.6 0.7 broadcast_in_dim.16
  1.3 0.7 maximum_bitcast_fusion
  2.0 3.0 %collective-permute-start.4 = (bf16[1,32,256]{2,1,0:T(8,128)(2,1)S(1)}, bf16[1,32,256]{2,1,0:T(8,128)(2,1)S(1)}, u32[]{:S(2)}, u32[]{:S(2)}) collective-permute-start(bf16[1,32,256]{2,1,0:T(8,128)(2,1)S(1)} %maximum_bitcast_fusion), channel_id=1, source_target_pairs={{0,4},{4,0},{8,12},{12,8},{16,20},{20,16},{24,28},{28,24},{1,5},{5... | collective-permute-start | bytes 49160 | tf_op jit(solution)/shard_map/ppermute | solution.py:264
  5.0 1.7 %collective-permute-done.4 = bf16[1,32,256]{2,1,0:T(8,128)(2,1)S(1)} collective-permute-done((bf16[1,32,256]{2,1,0:T(8,128)(2,1)S(1)}, bf16[1,32,256]{2,1,0:T(8,128)(2,1)S(1)}, u32[]{:S(2)}, u32[]{:S(2)}) %collective-permute-start.4) | collective-permute-done | bytes 16416 | tf_op jit(solution)/shard_map/ppermute | solution.py:264
  6.7 2.1 %collective-permute-start.5 = (bf16[2,32,256]{2,1,0:T(8,128)(2,1)S(1)}, bf16[2,32,256]{2,1,0:T(8,128)(2,1)S(1)}, u32[]{:S(2)}, u32[]{:S(2)}) collective-permute-start(bf16[2,32,256]{2,1,0:T(8,128)(2,1)S(1)} %maximum_select_fusion.4), channel_id=1, source_target_pairs={{0,8},{4,12},{8,0},{12,4},{16,24},{20,28},{24,16},{28,20},{1,9},{5... | collective-permute-start | bytes 98312 | tf_op jit(solution)/shard_map/ppermute | solution.py:264
  8.9 1.9 %collective-permute-done.5 = bf16[2,32,256]{2,1,0:T(8,128)(2,1)S(1)} collective-permute-done((bf16[2,32,256]{2,1,0:T(8,128)(2,1)S(1)}, bf16[2,32,256]{2,1,0:T(8,128)(2,1)S(1)}, u32[]{:S(2)}, u32[]{:S(2)}) %collective-permute-start.5) | collective-permute-done | bytes 32800 | tf_op jit(solution)/shard_map/ppermute | solution.py:264
  10.8 3.1 %collective-permute-start.6 = (bf16[4,32,256]{2,1,0:T(8,128)(2,1)S(1)}, bf16[4,32,256]{2,1,0:T(8,128)(2,1)S(1)}, u32[]{:S(2)}, u32[]{:S(2)}) collective-permute-start(bf16[4,32,256]{2,1,0:T(8,128)(2,1)S(1)} %maximum_select_fusion.3), channel_id=1, source_target_pairs={{0,16},{4,20},{8,24},{12,28},{16,0},{20,4},{24,8},{28,12},{1,17},{... | collective-permute-start | bytes 196616 | tf_op jit(solution)/shard_map/ppermute | solution.py:264
  13.9 1.0 fusion.5
  14.9 3.4 %collective-permute-start.3 = (bf16[32,2048]{1,0:T(8,128)(2,1)S(1)}, bf16[32,2048]{1,0:T(8,128)(2,1)S(1)}, u32[]{:S(2)}, u32[]{:S(2)}) collective-permute-start(bf16[32,2048]{1,0:T(8,128)(2,1)S(1)} %fusion.5), channel_id=1, source_target_pairs={{0,4},{4,8},{8,12},{12,16},{16,20},{20,24},{24,28},{1,5},{5,9},{9,... | collective-permute-start | bytes 393224 | tf_op jit(solution)/shard_map/ppermute | solution.py:270
  18.4 1.6 collective-permute-start.1
  20.0 0.7 pad_maximum_fusion
  20.9 0.7 copy-done.3
  21.5 11.1 %forward.1 = (bf16[256,2048]{1,0:T(8,128)(2,1)}, f32[16,256,128]{2,1,0:T(8,128)}, bf16[256,2048]{1,0:T(8,128)(2,1)}, f32[256,128]{1,0:T(8,128)}) custom-call(bf16[256,2048]{1,0:T(8,128)(2,1)} %bitcast.60, bf16[256,2048]{1,0:T(8,128)(2,1)} %bitcast.62, bf16[32,2048]{1,0:T(8,128)(2,1)} %copy-done.3, f32[16,32,128]{2,1,0:T(8,128)} %bitcast.64), custom_call_target="tpu_custom_call" | custom-call | flops 52428800 | bytes 6291456 | tf_op jit(solution)/shard_map/forward/pallas_call | solution.py:77
  32.7 1.8 %reshape.63 = bf16[256,8,2,128]{3,2,1,0:T(2,128)(2,1)S(1)} reshape(bf16[256,2048]{1,0:T(8,128)(2,1)} %get-tuple-element.18) | data formatting | bytes 2097152 | tf_op jit(solution)/shard_map/reshape | solution.py:358
  34.5 2.2 %constant_dynamic-slice_fusion = (bf16[256,8,1,128]{3,2,1,0:T(2,128)(2,1)S(1)}, bf16[256,8,1,128]{3,2,1,0:T(2,128)(2,1)S(1)}) fusion(bf16[256,8,2,128]{3,2,1,0:T(2,128)(2,1)S(1)} %reshape.63, s32[]{:T(128)S(6)} %select_n.116, s32[]{:T(128)S(6)} %select_n.115), kind=kLoop, calls=%fused_computation.29 | loop fusion | bytes 2097160 | tf_op jit(solution)/shard_map/jit(dynamic_index_in_dim)/dynamic_slice | solution.py:361
  36.6 2.0 %copy.25 = bf16[256,8,1,128]{0,3,1,2:T(8,128)(2,1)} copy(bf16[256,8,1,128]{3,2,1,0:T(2,128)(2,1)S(1)} %get-tuple-element.21) | data formatting | bytes 1048576
  38.6 1.5 collective-permute-start.8
  40.1 0.9 copy.24
  41.0 2.5 %fusion.6 = f32[1024,2048]{1,0:T(8,128)S(1)} fusion(bf16[256,1024]{0,1:T(8,128)(2,1)S(1)} %bitcast.67, bf16[1,256,2048]{2,1,0:T(8,128)(2,1)} %param.6), kind=kOutput, calls=%fused_computation.33 | convolution fusion | flops 1073741824 | bytes 9961472 | tf_op jit(solution)/shard_map/dot_general | solution.py:368
  43.5 8.4 %collective-permute-done.8 = bf16[256,1024]{0,1:T(8,128)(2,1)S(1)} collective-permute-done((bf16[256,1024]{0,1:T(8,128)(2,1)}, bf16[256,1024]{0,1:T(8,128)(2,1)S(1)}, u32[]{:S(2)}, u32[]{:S(2)}) %collective-permute-start.8) | collective-permute-done | bytes 524320 | tf_op jit(solution)/shard_map/ppermute | solution.py:255
  51.9 2.5 %convolution_add_fusion = f32[1024,2048]{1,0:T(8,128)S(1)} fusion(f32[1024,2048]{1,0:T(8,128)S(1)} %fusion.6, bf16[256,1024]{0,1:T(8,128)(2,1)S(1)} %collective-permute-done.8, bf16[256,2048]{1,0:T(8,128)(2,1)} %collective-permute-done.1), kind=kOutput, calls=%fused_computation | convolution fusion | flops 1075838976 | bytes 18350080 | tf_op jit(solution)/shard_map/dot_general | solution.py:368
  54.4 3.2 %copy-done = f32[1024,2048]{1,0:T(8,128)} copy-done((f32[1024,2048]{1,0:T(8,128)}, f32[1024,2048]{1,0:T(8,128)S(1)}, u32[]{:S(2)}) %copy-start) | copy-done | bytes 8388632
  58.9 2.3 %convolution_convert_fusion.3 = bf16[256,512]{1,0:T(8,128)(2,1)S(1)} fusion(bf16[512,2048]{1,0:T(8,128)(2,1)} %param.9, bf16[1,256,2048]{2,1,0:T(8,128)(2,1)S(1)} %copy-done.2), kind=kOutput, calls=%fused_computation.9 | convolution fusion | flops 537001984 | bytes 3407872 | tf_op jit(solution)/shard_map/dot_general | solution.py:329
  61.2 1.1 collective-permute-done.9
  62.3 3.4 %bitcast_add_fusion = f32[8,64,2048]{2,1,0:T(8,128)S(1)} fusion(bf16[8,64,2048]{2,1,0:T(8,128)(2,1)} %collective-permute-done.9, f32[8,2,64,2048]{3,2,1,0:T(8,128)} %bitcast.55, s32[]{:T(128)S(6)} %select_n.117), kind=kLoop, calls=%fused_computation.2 | loop fusion | flops 2097152 | bytes 10485764 | tf_op jit(solution)/shard_map/add | solution.py:376
  65.9 1.6 collective-permute-start.10
  67.5 2.7 %convolution_convert_fusion.1 = bf16[256,512]{1,0:T(8,128)(2,1)S(1)} fusion(bf16[256,2048]{1,0:T(8,128)(2,1)} %collective-permute-done.1, bf16[512,2048]{1,0:T(8,128)(2,1)} %param.9), kind=kOutput, calls=%fused_computation.7 | convolution fusion | flops 537001984 | bytes 3407872 | tf_op jit(solution)/shard_map/dot_general | solution.py:329
  70.2 2.7 %convolution_convert_fusion = bf16[256,512]{1,0:T(8,128)(2,1)S(1)} fusion(bf16[256,2048]{1,0:T(8,128)(2,1)} %collective-permute-done.1, bf16[512,2048]{1,0:T(8,128)(2,1)} %collective-permute-done), kind=kOutput, calls=%fused_computation.6 | convolution fusion | flops 537001984 | bytes 3407872 | tf_op jit(solution)/shard_map/dot_general | solution.py:333
  73.0 1.6 collective-permute-start.2
  74.5 2.3 %convolution_convert_fusion.2 = bf16[256,512]{1,0:T(8,128)(2,1)S(1)} fusion(bf16[512,2048]{1,0:T(8,128)(2,1)} %collective-permute-done, bf16[1,256,2048]{2,1,0:T(8,128)(2,1)S(1)} %copy-done.2), kind=kOutput, calls=%fused_computation.8 | convolution fusion | flops 537001984 | bytes 3407872 | tf_op jit(solution)/shard_map/dot_general | solution.py:333
  77.2 14.0 %collective-permute-done.10 = bf16[4,64,2048]{2,1,0:T(8,128)(2,1)S(1)} collective-permute-done((bf16[4,64,2048]{2,1,0:T(8,128)(2,1)S(1)}, bf16[4,64,2048]{2,1,0:T(8,128)(2,1)S(1)}, u32[]{:S(2)}, u32[]{:S(2)}) %collective-permute-start.10) | collective-permute-done | bytes 1048608 | tf_op jit(solution)/shard_map/ppermute | solution.py:264
  91.5 0.9 fusion.2
  92.3 1.6 collective-permute-start.11
  94.0 1.0 copy-done.1
  94.9 5.7 %normed_back.1 = (f32[16,256,128]{2,1,0:T(8,128)}, f32[8,2048]{1,0:T(8,128)}) custom-call(bf16[256,2048]{1,0:T(8,128)(2,1)} %copy-done.1, f32[16,256,128]{2,1,0:T(8,128)} %get-tuple-element.13.centred, f32[256,128]{1,0:T(8,128)} %get-tuple-element.14.inv, f32[16,32,128]{2,1,0:T(8,128)} %bitcast.65), custom_call_target="tpu_custom_call" | custom-call | flops 20971520 | bytes 5242880 | tf_op jit(solution)/shard_map/normed_back/pallas_call | solution.py:148
  100.7 12.1 %taps_back.1 = f32[32,2048]{1,0:T(8,128)} custom-call(f32[16,256,128]{2,1,0:T(8,128)} %get-tuple-element.15.grad_conv, bf16[256,2048]{1,0:T(8,128)(2,1)} %get-tuple-element.19.gated, bf16[32,2048]{1,0:T(8,128)(2,1)} %copy-done.3, f32[8,2048]{1,0:T(8,128)} %get-tuple-element.20.gain_part), custom_call_target="tpu_custom_call" | custom-call | flops 32505856 | bytes 3145728 | tf_op jit(solution)/shard_map/taps_back/pallas_call | solution.py:188
  112.7 1.7 %copy.29 = f32[4,8,8,256]{3,2,0,1:T(8,128)} copy(f32[4,8,8,256]{3,2,1,0:T(8,128)} %bitcast.69) | data formatting | bytes 524288 | tf_op jit(solution)/shard_map/all_to_all | solution.py:384
  114.4 3.4 %all-to-all-start = ((f32[32,8,256]{2,0,1:T(8,128)}), f32[32,8,256]{2,0,1:T(8,128)S(1)}, u32[]{:S(2)}, u32[]{:S(2)}) async-start(f32[32,8,256]{2,0,1:T(8,128)} %bitcast.53), calls=%async_computation | async-start | bytes 524288 | tf_op jit(solution)/shard_map/all_to_all | solution.py:384
  117.8 1.0 slice.27
  118.8 1.3 collective-permute-start.7
  120.1 9.2 %collective-permute-done.7.after = f32[16,32,128]{2,1,0:T(8,128)S(1)} collective-permute-done((f32[16,32,128]{2,1,0:T(8,128)S(1)}, f32[16,32,128]{2,1,0:T(8,128)S(1)}, u32[]{:S(2)}, u32[]{:S(2)}) %collective-permute-start.7) | collective-permute-done | bytes 262176 | tf_op jit(solution)/shard_map/ppermute | solution.py:270
  129.3 0.7 copy-done.4
  130.0 12.3 %gated_back.1 = (bf16[256,2048]{1,0:T(8,128)(2,1)}, bf16[256,2048]{1,0:T(8,128)(2,1)}) custom-call(f32[16,256,128]{2,1,0:T(8,128)} %get-tuple-element.15.grad_conv, f32[16,32,128]{2,1,0:T(8,128)} %copy-done.4, f32[16,32,128]{2,1,0:T(8,128)} %bitcast.66, bf16[256,2048]{1,0:T(8,128)(2,1)} %bitcast.61, bf16[256,2048]{1,0:T(8,128)(2,1)} %bitcast.63), custom_call_target="tpu_custom_call" | custom-call | flops 39321600 | bytes 6291456 | tf_op jit(solution)/shard_map/gated_back/pallas_call | solution.py:229
  142.3 5.4 %all-gather = f32[128,256]{1,0:T(8,128)S(1)} all-gather(f32[32,256]{1,0:T(8,128)S(1)} %reduce_sum.18), channel_id=2, replica_groups=mesh['sp'=8,'dp'=4] {'dp'}, dimensions={0}, use_global_device_ids=true | all-gather | bytes 163840 | tf_op jit(solution)/shard_map/all_gather | solution.py:386
  147.7 1.2 bitcast_add_fusion.2
  149.0 2.3 %collective-permute-start.12 = (bf16[1,64,2048]{2,1,0:T(8,128)(2,1)S(1)}, bf16[1,64,2048]{2,1,0:T(8,128)(2,1)S(1)}, u32[]{:S(2)}, u32[]{:S(2)}) collective-permute-start(bf16[1,64,2048]{2,1,0:T(8,128)(2,1)S(1)} %dynamic-slice_convert_fusion.2), channel_id=1, source_target_pairs={{0,16},{4,20},{8,24},{12,28},{16,0},{20,4},{24,8},{28,12},{1,17},{... | collective-permute-start | bytes 786440 | tf_op jit(solution)/shard_map/ppermute | solution.py:264
  152.5 11.6 %collective-permute-done.12 = bf16[1,64,2048]{2,1,0:T(8,128)(2,1)S(1)} collective-permute-done((bf16[1,64,2048]{2,1,0:T(8,128)(2,1)S(1)}, bf16[1,64,2048]{2,1,0:T(8,128)(2,1)S(1)}, u32[]{:S(2)}, u32[]{:S(2)}) %collective-permute-start.12) | collective-permute-done | bytes 262176 | tf_op jit(solution)/shard_map/ppermute | solution.py:264
  164.1 0.9 multiply_bitcast_fusion
  (31 shorter events, 3.6 us)
Async XLA Ops:
  2.0 4.7 %collective-permute-start.4 = (bf16[1,32,256]{2,1,0:T(8,128)(2,1)S(1)}, bf16[1,32,256]{2,1,0:T(8,128)(2,1)S(1)}, u32[]{:S(2)}, u32[]{:S(2)}) collective-permute-start(bf16[1,32,256]{2,1,0:T(8,128)(2,1)S(1)} %maximum_bitcast_fusion), channel_id=1, source_target_pairs={{0,4},{4,0},{8,12},{12,8},{16,20},{20,16},{24,28},{28,24},{1,5},{5... | collective-permute-start | bytes 49160 | tf_op jit(solution)/shard_map/ppermute | solution.py:264
  6.7 4.0 %collective-permute-start.5 = (bf16[2,32,256]{2,1,0:T(8,128)(2,1)S(1)}, bf16[2,32,256]{2,1,0:T(8,128)(2,1)S(1)}, u32[]{:S(2)}, u32[]{:S(2)}) collective-permute-start(bf16[2,32,256]{2,1,0:T(8,128)(2,1)S(1)} %maximum_select_fusion.4), channel_id=1, source_target_pairs={{0,8},{4,12},{8,0},{12,4},{16,24},{20,28},{24,16},{28,20},{1,9},{5... | collective-permute-start | bytes 98312 | tf_op jit(solution)/shard_map/ppermute | solution.py:264
  10.8 9.1 %collective-permute-start.6 = (bf16[4,32,256]{2,1,0:T(8,128)(2,1)S(1)}, bf16[4,32,256]{2,1,0:T(8,128)(2,1)S(1)}, u32[]{:S(2)}, u32[]{:S(2)}) collective-permute-start(bf16[4,32,256]{2,1,0:T(8,128)(2,1)S(1)} %maximum_select_fusion.3), channel_id=1, source_target_pairs={{0,16},{4,20},{8,24},{12,28},{16,0},{20,4},{24,8},{28,12},{1,17},{... | collective-permute-start | bytes 196616 | tf_op jit(solution)/shard_map/ppermute | solution.py:264
  14.9 5.9 %collective-permute-start.3 = (bf16[32,2048]{1,0:T(8,128)(2,1)S(1)}, bf16[32,2048]{1,0:T(8,128)(2,1)S(1)}, u32[]{:S(2)}, u32[]{:S(2)}) collective-permute-start(bf16[32,2048]{1,0:T(8,128)(2,1)S(1)} %fusion.5), channel_id=1, source_target_pairs={{0,4},{4,8},{8,12},{12,16},{16,20},{20,24},{24,28},{1,5},{5,9},{9,... | collective-permute-start | bytes 393224 | tf_op jit(solution)/shard_map/ppermute | solution.py:270
  18.4 33.6 %collective-permute-start.1 = (bf16[256,2048]{1,0:T(8,128)(2,1)}, bf16[256,2048]{1,0:T(8,128)(2,1)}, u32[]{:S(2)}, u32[]{:S(2)}) collective-permute-start(bf16[256,2048]{1,0:T(8,128)(2,1)} %bitcast.68), channel_id=1, source_target_pairs={{0,2},{1,3},{2,0},{3,1},{4,6},{5,7},{6,4},{7,5},{8,10},{9,11},{10,... | collective-permute-start | bytes 3145736 | tf_op jit(solution)/shard_map/ppermute | solution.py:255
  20.9 0.7 copy-start.3
  38.6 13.3 %collective-permute-start.8 = (bf16[256,1024]{0,1:T(8,128)(2,1)}, bf16[256,1024]{0,1:T(8,128)(2,1)S(1)}, u32[]{:S(2)}, u32[]{:S(2)}) collective-permute-start(bf16[256,1024]{0,1:T(8,128)(2,1)} %bitcast.9), channel_id=1, source_target_pairs={{0,2},{1,3},{2,0},{3,1},{4,6},{5,7},{6,4},{7,5},{8,10},{9,11},{10,... | collective-permute-start | bytes 1572872 | tf_op jit(solution)/shard_map/ppermute | solution.py:255
  54.4 3.2 %copy-start = (f32[1024,2048]{1,0:T(8,128)}, f32[1024,2048]{1,0:T(8,128)S(1)}, u32[]{:S(2)}) copy-start(f32[1024,2048]{1,0:T(8,128)S(1)} %convolution_add_fusion) | copy-start | bytes 25165828
  57.7 1.2 copy-start.2
  58.0 4.4 %collective-permute-start.9 = (bf16[8,64,2048]{2,1,0:T(8,128)(2,1)S(1)}, bf16[8,64,2048]{2,1,0:T(8,128)(2,1)}, u32[]{:S(2)}, u32[]{:S(2)}) collective-permute-start(bf16[8,64,2048]{2,1,0:T(8,128)(2,1)S(1)} %fusion), channel_id=1, source_target_pairs={{0,1},{1,0},{2,3},{3,2},{4,5},{5,4},{6,7},{7,6},{8,9},{9,8},{10,11... | collective-permute-start | bytes 6291464 | tf_op jit(solution)/shard_map/ppermute | solution.py:259
  58.0 12.1 %collective-permute-start = (bf16[512,2048]{1,0:T(8,128)(2,1)}, bf16[512,2048]{1,0:T(8,128)(2,1)}, u32[]{:S(2)}, u32[]{:S(2)}) collective-permute-start(bf16[512,2048]{1,0:T(8,128)(2,1)} %param.9), channel_id=1, source_target_pairs={{0,1},{1,0},{2,3},{3,2},{4,5},{5,4},{6,7},{7,6},{8,9},{9,8},{10,11... | collective-permute-start | bytes 6291464 | tf_op jit(solution)/shard_map/ppermute | solution.py:259
  65.9 25.3 %collective-permute-start.10 = (bf16[4,64,2048]{2,1,0:T(8,128)(2,1)S(1)}, bf16[4,64,2048]{2,1,0:T(8,128)(2,1)S(1)}, u32[]{:S(2)}, u32[]{:S(2)}) collective-permute-start(bf16[4,64,2048]{2,1,0:T(8,128)(2,1)S(1)} %fusion.1), channel_id=1, source_target_pairs={{0,4},{4,0},{8,12},{12,8},{16,20},{20,16},{24,28},{28,24},{1,5},{5... | collective-permute-start | bytes 3145736 | tf_op jit(solution)/shard_map/ppermute | solution.py:264
  73.0 20.9 %collective-permute-start.2 = (bf16[256,1024]{1,0:T(8,128)(2,1)S(1)}, bf16[256,1024]{1,0:T(8,128)(2,1)S(1)}, u32[]{:S(2)}, u32[]{:S(2)}) collective-permute-start(bf16[256,1024]{1,0:T(8,128)(2,1)S(1)} %maximum_select_fusion.1), channel_id=1, source_target_pairs={{0,2},{1,3},{2,0},{3,1},{4,6},{5,7},{6,4},{7,5},{8,10},{9,11},{10,... | collective-permute-start | bytes 1572872 | tf_op jit(solution)/shard_map/ppermute | solution.py:255
  92.3 55.4 %collective-permute-start.11 = (bf16[2,64,2048]{2,1,0:T(8,128)(2,1)}, bf16[2,64,2048]{2,1,0:T(8,128)(2,1)}, u32[]{:S(2)}, u32[]{:S(2)}) collective-permute-start(bf16[2,64,2048]{2,1,0:T(8,128)(2,1)} %fusion.2), channel_id=1, source_target_pairs={{0,8},{4,12},{8,0},{12,4},{16,24},{20,28},{24,16},{28,20},{1,9},{5... | collective-permute-start | bytes 1572872 | tf_op jit(solution)/shard_map/ppermute | solution.py:264
  94.0 1.0 copy-start.1
  114.4 27.9 %all-to-all-start = ((f32[32,8,256]{2,0,1:T(8,128)}), f32[32,8,256]{2,0,1:T(8,128)S(1)}, u32[]{:S(2)}, u32[]{:S(2)}) async-start(f32[32,8,256]{2,0,1:T(8,128)} %bitcast.53), calls=%async_computation | async-start | bytes 524288 | tf_op jit(solution)/shard_map/all_to_all | solution.py:384
  118.8 10.5 %collective-permute-start.7 = (f32[16,32,128]{2,1,0:T(8,128)S(1)}, f32[16,32,128]{2,1,0:T(8,128)S(1)}, u32[]{:S(2)}, u32[]{:S(2)}) collective-permute-start(f32[16,32,128]{2,1,0:T(8,128)S(1)} %slice.27), channel_id=1, source_target_pairs={{4,0},{8,4},{12,8},{16,12},{20,16},{24,20},{28,24},{5,1},{9,5},{13... | collective-permute-start | bytes 786440 | tf_op jit(solution)/shard_map/ppermute | solution.py:270
  129.3 0.7 copy-start.4
  149.0 15.1 %collective-permute-start.12 = (bf16[1,64,2048]{2,1,0:T(8,128)(2,1)S(1)}, bf16[1,64,2048]{2,1,0:T(8,128)(2,1)S(1)}, u32[]{:S(2)}, u32[]{:S(2)}) collective-permute-start(bf16[1,64,2048]{2,1,0:T(8,128)(2,1)S(1)} %dynamic-slice_convert_fusion.2), channel_id=1, source_target_pairs={{0,16},{4,20},{8,24},{12,28},{16,0},{20,4},{24,8},{28,12},{1,17},{... | collective-permute-start | bytes 786440 | tf_op jit(solution)/shard_map/ppermute | solution.py:264
